TPU v7x, 32 devices: a whole 2x2x4 slice. The times are simulated.
32 devices in a mesh: ep: 8 (over z, x), tp: 4 (over y, core).
Axes of the slice: x: 2, y: 2, z: 4, core: 2. Of those that a mesh axis runs over, the one named last changes fastest.
Arguments:
- query_latent: bfloat16 [2048, 512], P(('ep', 'tp')), may hold values from -6 to 6
- key_latent: bfloat16 [2048, 256], P(('ep', 'tp')), may hold values from -6 to 6
- rotary_key: bfloat16 [2048, 32], P(('ep', 'tp')), may hold values from -140 to 140
- query_gain: float32 [512], replicated, may hold values from 0.1 to 1.9
- latent_gain: float32 [256], replicated, may hold values from 0.1 to 1.9
- query_content: bfloat16 [512, 512], replicated, may hold values from -0.625 to 0.625
- query_rotary: bfloat16 [512, 256], replicated, may hold values from -0.625 to 0.625
- key_content: bfloat16 [256, 512], replicated, may hold values from -0.375 to 0.375
- value_weight: bfloat16 [256, 512], replicated, may hold values from -0.375 to 0.375
- output_weight: bfloat16 [512, 2048], P('tp'), may hold values from -1 to 1
- expert_input: bfloat16 [2048, 2048], P(('ep', 'tp')), may hold values from -6 to 6
- norm_gain: float32 [2048], replicated, may hold values from 0.1 to 1.9
- routes: int32 [2048, 2], P(('ep', 'tp')), may hold values from 0 to 15, all different within a row; in each aligned block of 64 rows (0 to 63, 64 to 127, ...) at most 16 rows name the same one
- route_weight: float32 [2048, 2], P(('ep', 'tp')), may hold values from 0.25 to 2
- expert_gate: bfloat16 [16, 2048, 1024], P('ep', None, 'tp'), may hold values from -0.125 to 0.125
- expert_up: bfloat16 [16, 2048, 1024], P('ep', None, 'tp'), may hold values from -0.125 to 0.125
- expert_down: bfloat16 [16, 1024, 2048], P('ep', 'tp'), may hold values from -0.1875 to 0.1875
- shared_gate: bfloat16 [2048, 1024], P(None, 'tp'), may hold values from -0.125 to 0.125
- shared_up: bfloat16 [2048, 1024], P(None, 'tp'), may hold values from -0.125 to 0.125
- shared_down: bfloat16 [1024, 2048], P('tp'), may hold values from -0.1875 to 0.1875
Outputs:
- mixer_out: bfloat16 [2048, 2048], P(('ep', 'tp'))
- expert_out: bfloat16 [2048, 2048], P(('ep', 'tp'))
Inputs may be any that keep to these rules, and one draw needn't show every extreme that they name: `routes`: each row names 2 different experts. Within the rows of one device (aligned blocks of 64 rows) no expert is named by more than 16 rows, and in every draw some expert is named by exactly 16 rows of some device.
All inputs are finite; a program needn't handle non-finite values.
Results may differ from a plain program's by a relative error of at most 0.013.
The roundings to bfloat16 on the way count: a program that leaves them out, or rounds other values in their place, can miss the bound.
Values may be sent and summed in bfloat16 or wider, within the bound.
A program may use at most 128 MiB of HBM per device.

v0:
```python
import math

import jax
import jax.numpy as jnp
from jax import lax
from jax.sharding import PartitionSpec as P

HEADS = 8
CONTENT = 64
ROTARY = 32
VALUE = 64


norm_eps = 1e-06
rope_base = 10000.0


def rms_rows(entries, gain_row):
    widened = entries.astype(jnp.float32)
    return widened * lax.rsqrt(jnp.mean(widened * widened, -1, keepdims=True) + norm_eps) * gain_row


def turn_pairs(entries, positions):
    width_full = entries.shape[-1]
    frequency = rope_base ** (-jnp.arange(width_full // 2, dtype=jnp.float32) * 2.0 / width_full)
    angles = positions.astype(jnp.float32)[:, None] * frequency[None, :]
    cosine = jnp.cos(angles)[:, None, :]
    sine_part = jnp.sin(angles)[:, None, :]
    even_part = entries[..., 0::2]
    odd_part = entries[..., 1::2]
    joined = jnp.stack(
        [even_part * cosine - odd_part * sine_part, even_part * sine_part + odd_part * cosine], -1
    )
    return joined.reshape(entries.shape)


def absorb_block(carried, query_part, query_turn, key_part, key_turn, value_rows, score_scale):
    running_peak, running_total, summed = carried
    scores = jnp.einsum("qhc,khc->qhk", query_part, key_part, preferred_element_type=jnp.float32)
    scores = scores + jnp.einsum(
        "qhr,kr->qhk", query_turn, key_turn, preferred_element_type=jnp.float32
    )
    scores = scores * score_scale
    new_peak = jnp.maximum(running_peak, jnp.max(scores, -1))
    factor = jnp.exp(running_peak - new_peak)
    weights = jnp.exp(scores - new_peak[..., None])
    running_total = running_total * factor + jnp.sum(weights, -1)
    summed = summed * factor[..., None] + jnp.einsum(
        "qhk,khv->qhv", weights.astype(jnp.bfloat16), value_rows, preferred_element_type=jnp.float32
    )
    return (new_peak, running_total, summed)


def absorb_piece(carried, query_part, query_turn, key_part, key_turn, value_rows, score_scale):
    row_count = key_part.shape[0]
    key_block = math.gcd(row_count, 2048)
    if key_block == row_count:
        return absorb_block(
            carried, query_part, query_turn, key_part, key_turn, value_rows, score_scale
        )
    block_count = row_count // key_block

    def advance(state, pieces):
        return (
            absorb_block(
                state, query_part, query_turn, pieces[0], pieces[1], pieces[2], score_scale
            ),
            None,
        )

    stacked = (
        key_part.reshape((block_count, key_block) + key_part.shape[1:]),
        key_turn.reshape(block_count, key_block, key_turn.shape[1]),
        value_rows.reshape((block_count, key_block) + value_rows.shape[1:]),
    )
    carried, ignored = lax.scan(advance, carried, stacked)
    return carried


def expand_keys(latent_rows, key_columns, value_columns, head_local):
    row_count = latent_rows.shape[0]
    key_part = (
        jnp.dot(latent_rows, key_columns, preferred_element_type=jnp.float32)
        .astype(jnp.bfloat16)
        .reshape(row_count, head_local, CONTENT)
    )
    value_rows = (
        jnp.dot(latent_rows, value_columns, preferred_element_type=jnp.float32)
        .astype(jnp.bfloat16)
        .reshape(row_count, head_local, VALUE)
    )
    return (key_part, value_rows)


def expert_terms(row_block, gate_weight, up_weight, down_weight):
    gated = jnp.einsum("secd,edf->secf", row_block, gate_weight, preferred_element_type=jnp.float32)
    lifted = jnp.einsum("secd,edf->secf", row_block, up_weight, preferred_element_type=jnp.float32)
    hidden = (jax.nn.silu(gated) * lifted).astype(jnp.bfloat16)
    return jnp.einsum("secf,efd->secd", hidden, down_weight, preferred_element_type=jnp.float32)


def shared_terms(row_block, gate_weight, up_weight, down_weight):
    gated = jnp.dot(row_block, gate_weight, preferred_element_type=jnp.float32)
    lifted = jnp.dot(row_block, up_weight, preferred_element_type=jnp.float32)
    hidden = (jax.nn.silu(gated) * lifted).astype(jnp.bfloat16)
    return jnp.dot(hidden, down_weight, preferred_element_type=jnp.float32)


def shards(
    query_latent,
    key_latent,
    rotary_key,
    query_gain,
    latent_gain,
    query_content,
    query_rotary,
    key_content,
    value_weight,
    output_weight,
    expert_input,
    norm_gain,
    routes,
    route_weight,
    expert_gate,
    expert_up,
    expert_down,
    shared_gate,
    shared_up,
    shared_down,
):
    group_size = lax.axis_size("tp")
    expert_groups = lax.axis_size("ep")
    own_rows = query_latent.shape[0]
    head_local = HEADS // group_size
    head_index = lax.axis_index("tp")
    group_rows_count = own_rows * group_size
    group_start = lax.axis_index("ep") * group_rows_count
    own_start = group_start + head_index * own_rows
    score_scale = (CONTENT + ROTARY) ** (-0.5)
    query_normed = rms_rows(query_latent, query_gain).astype(jnp.bfloat16)
    latent_normed = rms_rows(key_latent, latent_gain).astype(jnp.bfloat16)
    own_positions = own_start + jnp.arange(own_rows, dtype=jnp.int32)
    key_turned = turn_pairs(rotary_key.astype(jnp.float32)[:, None, :], own_positions)[
        :, 0, :
    ].astype(jnp.bfloat16)
    token_rows = expert_input.shape[0]
    picks = routes.shape[1]
    local_experts = expert_gate.shape[0]
    expert_total = local_experts * expert_groups
    capacity = 2 * token_rows * picks // expert_total
    slot_total = expert_total * capacity
    model_width = expert_input.shape[1]
    expert_normed = rms_rows(expert_input, norm_gain).astype(jnp.bfloat16)
    flat_routes = routes.reshape(-1)
    marks = (flat_routes[:, None] == jnp.arange(expert_total, dtype=jnp.int32)[None, :]).astype(
        jnp.int32
    )
    ranks = jnp.sum((jnp.cumsum(marks, 0) - marks) * marks, 1)
    targets = flat_routes * capacity + ranks
    picker = (jnp.arange(slot_total, dtype=jnp.int32)[:, None] == targets[None, :]).astype(
        jnp.int32
    )
    picker = jnp.sum(picker.reshape(slot_total, token_rows, picks), 2).astype(jnp.bfloat16)
    outgoing = jnp.dot(picker, expert_normed, preferred_element_type=jnp.float32).astype(
        jnp.bfloat16
    )
    outgoing = outgoing.reshape(expert_groups, local_experts, capacity, model_width)
    received = lax.all_to_all(outgoing, "ep", split_axis=0, concat_axis=0, tiled=True)
    group_query, group_latent, group_turn, gathered_rows, gathered_tokens = (
        lax.all_gather(query_normed, "tp", axis=0, tiled=True),
        lax.all_gather(latent_normed, "tp", axis=0, tiled=True),
        lax.all_gather(key_turned, "tp", axis=0, tiled=True),
        lax.all_gather(received, "tp", axis=0, tiled=True),
        lax.all_gather(expert_normed, "tp", axis=0, tiled=True),
    )
    positions = group_start + jnp.arange(group_rows_count, dtype=jnp.int32)
    content_columns = lax.dynamic_slice_in_dim(
        query_content, head_index * head_local * CONTENT, head_local * CONTENT, 1
    )
    rotary_columns = lax.dynamic_slice_in_dim(
        query_rotary, head_index * head_local * ROTARY, head_local * ROTARY, 1
    )
    query_part = (
        jnp.dot(group_query, content_columns, preferred_element_type=jnp.float32)
        .astype(jnp.bfloat16)
        .reshape(group_rows_count, head_local, CONTENT)
    )
    query_turn = turn_pairs(
        jnp.dot(group_query, rotary_columns, preferred_element_type=jnp.float32).reshape(
            group_rows_count, head_local, ROTARY
        ),
        positions,
    ).astype(jnp.bfloat16)
    key_columns = lax.dynamic_slice_in_dim(
        key_content, head_index * head_local * CONTENT, head_local * CONTENT, 1
    )
    value_columns = lax.dynamic_slice_in_dim(
        value_weight, head_index * head_local * VALUE, head_local * VALUE, 1
    )
    carry_start = (
        jnp.full((group_rows_count, head_local), -jnp.inf, jnp.float32),
        jnp.zeros((group_rows_count, head_local), jnp.float32),
        jnp.zeros((group_rows_count, head_local, VALUE), jnp.float32),
    )
    key_part, value_rows = expand_keys(
        lax.all_gather(group_latent, "ep", axis=0, tiled=True),
        key_columns,
        value_columns,
        head_local,
    )
    running_peak, running_total, summed = absorb_piece(
        carry_start,
        query_part,
        query_turn,
        key_part,
        lax.all_gather(group_turn, "ep", axis=0, tiled=True),
        value_rows,
        score_scale,
    )
    attended = (
        (summed / running_total[..., None])
        .astype(jnp.bfloat16)
        .reshape(group_rows_count, head_local * VALUE)
    )
    routed_term = expert_terms(gathered_rows, expert_gate, expert_up, expert_down)
    shared_term = shared_terms(gathered_tokens, shared_gate, shared_up, shared_down)
    mixer_term = jnp.dot(attended, output_weight, preferred_element_type=jnp.float32)
    mixer_sum, routed_sum, shared_sum = (
        lax.psum_scatter(
            mixer_term.astype(jnp.bfloat16), "tp", scatter_dimension=0, tiled=True
        ).astype(jnp.float32),
        lax.psum_scatter(
            routed_term.astype(jnp.bfloat16), "tp", scatter_dimension=0, tiled=True
        ).astype(jnp.float32),
        lax.psum_scatter(
            shared_term.astype(jnp.bfloat16), "tp", scatter_dimension=0, tiled=True
        ).astype(jnp.float32),
    )
    mixer_out = mixer_sum.astype(jnp.bfloat16)
    returned = lax.all_to_all(
        routed_sum.astype(jnp.bfloat16), "ep", split_axis=0, concat_axis=0, tiled=True
    )
    returned = returned.reshape(slot_total, model_width)
    picked = jnp.take(returned, targets, axis=0).reshape(token_rows, picks, model_width)
    combined = jnp.sum(route_weight[..., None] * picked.astype(jnp.float32), 1) + shared_sum
    expert_out = combined.astype(jnp.bfloat16)
    return (mixer_out, expert_out)


def solution(mesh):
    in_specs = (
        P(("ep", "tp"), None),
        P(("ep", "tp"), None),
        P(("ep", "tp"), None),
        P(),
        P(),
        P(),
        P(),
        P(),
        P(),
        P("tp", None),
        P(("ep", "tp"), None),
        P(),
        P(("ep", "tp"), None),
        P(("ep", "tp"), None),
        P("ep", None, "tp"),
        P("ep", None, "tp"),
        P("ep", "tp", None),
        P(None, "tp"),
        P(None, "tp"),
        P("tp", None),
    )
    out_specs = (P(("ep", "tp"), None), P(("ep", "tp"), None))
    return jax.shard_map(shards, mesh=mesh, in_specs=in_specs, out_specs=out_specs, check_vma=False)
```

profile of v0, /device:TPU:0, one launch (start us, length us, event | category | flops | bytes accessed | tf_op | source)
XLA Modules:
  0.0 250.2 jit_solution(3735502933003136153)
XLA Ops:
  13.4 32.8 %all_to_all.10 = bf16[8,2,16,2048]{3,2,1,0:T(8,128)(2,1)S(1)} all-to-all(bf16[8,2,16,2048]{3,2,1,0:T(8,128)(2,1)S(1)} %bitcast.114), channel_id=1, replica_groups=mesh['ep'=8,'tp'=4] {'ep'}, dimensions={0} | all-to-all | bytes 2097152 | tf_op jit(solution)/shard_map/all_to_all | solution.py:168
  48.4 5.9 %all_gather.21 = bf16[256,256]{1,0:T(8,128)(2,1)} all-gather(bf16[64,256]{1,0:T(8,128)(2,1)S(1)} %fusion.57), channel_id=1, replica_groups=mesh['ep'=8,'tp'=4] {'tp'}, dimensions={0}, use_global_device_ids=true | all-gather | bytes 163840 | tf_op jit(solution)/shard_map/all_gather | solution.py:171
  54.3 26.7 %all-gather.7.cloned.1.call-done = bf16[32,2,16,2048]{3,2,0,1:T(8,128)(2,1)} async-done(((bf16[8,2,16,2048]{3,2,0,1:T(8,128)(2,1)}), bf16[32,2,16,2048]{3,2,0,1:T(8,128)(2,1)}) %all-gather.7.cloned.1.call-update) | async-done | bytes 4194320 | tf_op jit(solution)/shard_map/all_gather | solution.py:173
  81.0 4.1 %fusion.11 = f32[32,2,16,256]{3,2,0,1:T(8,128)S(1)} fusion(bf16[32,2,16,2048]{3,2,0,1:T(8,128)(2,1)} %all-gather.7.cloned.1.call-done, bf16[2,2048,256]{2,1,0:T(8,128)(2,1)} %param.34), kind=kOutput, calls=%fused_computation.19 | convolution fusion | flops 1073741824 | bytes 7340032 | tf_op jit(solution)/shard_map/secd,edf->secf/dot_general | solution.py:96
  85.2 7.3 %convert_bitcast_fusion = bf16[32,2,16,2048]{3,2,0,1:T(8,128)(2,1)} fusion(bf16[2,256,2048]{2,1,0:T(8,128)(2,1)S(1)} %copy-done, bf16[32,2,16,2048]{3,2,0,1:T(8,128)(2,1)} %all-gather.7.cloned.1.call-done, bf16[2,2048,256]{2,1,0:T(8,128)(2,1)} %param.35, f32[32,2,16,256]{3,2,0,1:T(8,128)S(1)} %fusion.11), kind=kOutput, calls=%fused_computation.3 | convolution fusion | flops 2151153664 | bytes 13631488 | tf_op jit(solution)/shard_map/secf,efd->secd/dot_general | solution.py:99
  92.5 2.5 copy.77
  95.0 4.2 %copy.79 = bf16[4,8,32,2048]{3,1,2,0:T(8,128)(2,1)} copy(bf16[4,8,32,2048]{3,2,1,0:T(8,128)(2,1)S(1)} %bitcast.112) | data formatting | bytes 8388608
  100.3 5.8 %all_gather.23 = bf16[256,512]{1,0:T(8,128)(2,1)S(1)} all-gather(bf16[64,512]{1,0:T(8,128)(2,1)S(1)} %fusion.49), channel_id=1, replica_groups=mesh['ep'=8,'tp'=4] {'tp'}, dimensions={0}, use_global_device_ids=true | all-gather | bytes 327680 | tf_op jit(solution)/shard_map/all_gather | solution.py:170
  109.4 5.2 %all-gather = bf16[4,64,32]{1,2,0:T(8,128)(2,1)S(1)} all-gather(bf16[1,64,32]{1,2,0:T(8,128)(2,1)S(1)} %bitcast.122), channel_id=1, replica_groups=mesh['ep'=8,'tp'=4] {'tp'}, dimensions={0}, use_global_device_ids=true | all-gather | bytes 20480 | tf_op jit(solution)/shard_map/all_gather | solution.py:172
  114.7 31.1 %all_gather.25 = bf16[2048,32]{0,1:T(8,128)(2,1)S(1)} all-gather(bf16[256,32]{0,1:T(8,128)(2,1)S(1)} %reshape.292), channel_id=1, replica_groups=mesh['ep'=8,'tp'=4] {'ep'}, dimensions={0}, use_global_device_ids=true | all-gather | bytes 147456 | tf_op jit(solution)/shard_map/all_gather | solution.py:216
  145.8 1.8 convolution_convert_fusion.5
  147.6 2.4 fusion.86
  149.9 4.6 %convolution_convert_fusion.1 = bf16[256,2048]{1,0:T(8,128)(2,1)} fusion(bf16[256,2048]{1,0:T(8,128)(2,1)} %param.39, bf16[256,2048]{1,0:T(8,128)(2,1)} %all-gather.9.cloned.1.call-done, bf16[2048,256]{1,0:T(8,128)(2,1)} %param.38, f32[256,256]{1,0:T(8,128)} %fusion.86), kind=kOutput, calls=%fused_computation.8 | convolution fusion | flops 537788416 | bytes 4456448 | tf_op jit(solution)/shard_map/dot_general | solution.py:106
  154.6 1.8 convolution_convert_fusion.4
  157.9 2.0 copy-done.1
  160.4 2.1 convolution_convert_fusion.3
  162.6 25.8 %reduce-scatter.11.cloned.1.call-done = bf16[8,65536]{1,0:T(8,128)(2,1)} async-done(((bf16[32,65536]{1,0:T(8,128)(2,1)}), bf16[8,65536]{1,0:T(8,128)(2,1)}) %reduce-scatter.11.cloned.1.call-update) | async-done | bytes 1048592
  188.4 2.8 %copy.80 = bf16[1,8,32,2048]{3,2,1,0:T(8,128)(2,1)} copy(bf16[1,8,32,2048]{3,1,2,0:T(8,128)(2,1)} %bitcast.117) | data formatting | bytes 2097152
  191.1 5.5 %all-to-all-start.1 = ((bf16[8,2,16,2048]{3,2,1,0:T(8,128)(2,1)}), bf16[8,2,16,2048]{3,2,1,0:T(8,128)(2,1)S(1)}, u32[]{:S(2)}, u32[]{:S(2)}) async-start(bf16[8,2,16,2048]{3,2,1,0:T(8,128)(2,1)} %bitcast.113), calls=%async_computation.2 | async-start | bytes 2097152 | tf_op jit(solution)/shard_map/all_to_all | solution.py:240
  196.8 3.5 %fusion.33 = bf16[256,2,64]{0,2,1:T(8,128)(2,1)S(1)} fusion(bf16[2048,2,64]{0,2,1:T(8,128)(2,1)} %bitcast.115, f32[256,2,2048]{0,2,1:T(8,128)} %copy-done.1, f32[256,2]{0,1:T(2,128)S(1)} %get-tuple-element.12, f32[256,2]{0,1:T(2,128)S(1)} %get-tuple-element.9, f32[256,2]{0,1:T(2,128)S(1)} %get-tuple-element.8), kind=kOutput, calls=%fused_computation.28 | convolution fusion | flops 136413184 | bytes 4790272 | tf_op jit(solution)/shard_map/qhk,khv->qhv/dot_general | solution.py:48
  202.2 20.1 %all-to-all-done.1 = bf16[8,2,16,2048]{3,2,1,0:T(8,128)(2,1)S(1)} async-done(((bf16[8,2,16,2048]{3,2,1,0:T(8,128)(2,1)}), bf16[8,2,16,2048]{3,2,1,0:T(8,128)(2,1)S(1)}, u32[]{:S(2)}, u32[]{:S(2)}) %all-to-all-start.1) | async-done | bytes 1048608 | tf_op jit(solution)/shard_map/all_to_all | solution.py:240
  222.3 1.8 gather_fusion
  225.5 2.5 multiply_reduce_fusion
  229.7 13.7 %reduce-scatter.7.cloned.1.call-done = bf16[64,2048]{1,0:T(8,128)(2,1)} async-done(((bf16[256,2048]{1,0:T(8,128)(2,1)}), bf16[64,2048]{1,0:T(8,128)(2,1)}) %reduce-scatter.7.cloned.1.call-update) | async-done | bytes 262160 | tf_op jit(solution)/shard_map/reduce_scatter | solution.py:229
  (105 shorter events, 19.9 us)
Async XLA Ops:
  7.2 78.0 %copy-start = (bf16[2,256,2048]{2,1,0:T(8,128)(2,1)S(1)}, bf16[2,256,2048]{2,1,0:T(8,128)(2,1)}, u32[]{:S(2)}) copy-start(bf16[2,256,2048]{2,1,0:T(8,128)(2,1)} %param.36) | copy-start | bytes 6291460
  7.2 41.0 %copy-start.9 = (bf16[64,256]{1,0:T(8,128)(2,1)S(1)}, bf16[64,256]{1,0:T(8,128)(2,1)}, u32[]{:S(2)}) copy-start(bf16[64,256]{1,0:T(8,128)(2,1)} %param.21) | copy-start | bytes 98308
  7.2 41.1 %copy-start.17 = (f32[256]{0:T(256)S(1)}, f32[256]{0:T(256)}, u32[]{:S(2)}) copy-start(f32[256]{0:T(256)} %param.24) | copy-start | bytes 3076
  7.2 73.8 %all-gather.7.cloned.1.call-start = ((), (), s32[]{:S(2)}) async-start(), calls=%async_computation.7 | async-start | bytes 5242880 | tf_op jit(solution)/shard_map/all_gather | solution.py:173
  13.0 34.4 %copy-start.3 = (bf16[64,2048]{1,0:T(8,128)(2,1)}, bf16[64,2048]{1,0:T(8,128)(2,1)S(1)}, u32[]{:S(2)}) copy-start(bf16[64,2048]{1,0:T(8,128)(2,1)S(1)} %fusion.40) | copy-start | bytes 786436
  47.4 100.2 %all-gather.9.cloned.1.call-start = ((), (), s32[]{:S(2)}) async-start(), calls=%async_computation.8 | async-start | bytes 1310720 | tf_op jit(solution)/shard_map/all_gather | solution.py:174
  48.1 106.4 %all-gather.5.cloned.1.call-start = ((), (), s32[]{:S(2)}) async-start(), calls=%async_computation.5 | async-start | bytes 1179648 | tf_op jit(solution)/shard_map/all_gather | solution.py:206
  54.3 134.1 %reduce-scatter.11.cloned.1.call-start = ((), (), s32[]{:S(2)}) async-start(), calls=%async_computation.10 | async-start | bytes 5242880
  99.2 0.8 copy-start.7
  99.2 1.0 copy-start.12
  99.2 8.1 %copy-start.11 = (bf16[64,32]{0,1:T(8,128)(2,1)S(1)}, bf16[64,32]{0,1:T(8,128)(2,1)}, u32[]{:S(2)}) copy-start(bf16[64,32]{0,1:T(8,128)(2,1)} %param.22) | copy-start | bytes 12292
  99.2 48.3 %copy-start.4 = (bf16[2048,256]{1,0:T(8,128)(2,1)S(1)}, bf16[2048,256]{1,0:T(8,128)(2,1)}, u32[]{:S(2)}) copy-start(bf16[2048,256]{1,0:T(8,128)(2,1)} %param.37) | copy-start | bytes 3145732
  99.3 128.7 %reduce-scatter.9.cloned.1.call-start = ((), (), s32[]{:S(2)}) async-start(), calls=%async_computation.9 | async-start | bytes 1310720 | tf_op jit(solution)/shard_map/reduce_scatter | solution.py:235
  149.9 6.4 %copy-start.6 = (bf16[256,128]{0,1:T(8,128)(2,1)S(1)}, bf16[256,128]{0,1:T(8,128)(2,1)}, u32[]{:S(2)}) copy-start(bf16[256,128]{0,1:T(8,128)(2,1)} %convolution_convert_fusion.5) | copy-start | bytes 196612
  154.5 2.6 %copy-start.8 = (bf16[256,2,32]{0,2,1:T(8,128)(2,1)S(1)}, bf16[256,2,32]{0,2,1:T(8,128)(2,1)}, u32[]{:S(2)}) copy-start(bf16[256,2,32]{0,2,1:T(8,128)(2,1)} %convert_element_type.107) | copy-start | bytes 98308
  157.9 2.0 copy-start.1
  157.9 2.5 %copy-start.2 = (bf16[2048,256]{1,0:T(8,128)(2,1)S(1)}, bf16[2048,256]{1,0:T(8,128)(2,1)}, u32[]{:S(2)}) copy-start(bf16[2048,256]{1,0:T(8,128)(2,1)} %all-gather.5.cloned.1.call-done) | copy-start | bytes 3145732
  191.1 31.2 %all-to-all-start.1 = ((bf16[8,2,16,2048]{3,2,1,0:T(8,128)(2,1)}), bf16[8,2,16,2048]{3,2,1,0:T(8,128)(2,1)S(1)}, u32[]{:S(2)}, u32[]{:S(2)}) async-start(bf16[8,2,16,2048]{3,2,1,0:T(8,128)(2,1)} %bitcast.113), calls=%async_computation.2 | async-start | bytes 2097152 | tf_op jit(solution)/shard_map/all_to_all | solution.py:240
  196.7 5.0 %copy-start.10 = (s32[64,2]{0,1:T(2,128)S(1)}, s32[64,2]{0,1:T(2,128)}, u32[]{:S(2)}) copy-start(s32[64,2]{0,1:T(2,128)} %param.32) | copy-start | bytes 1540
  196.7 5.3 %copy-start.16 = (pred[64,2]{0,1:T(4,128)(4,1)S(1)}, pred[64,2]{0,1:T(4,128)(4,1)}, u32[]{:S(2)}) copy-start(pred[64,2]{0,1:T(4,128)(4,1)} %get-tuple-element.2) | copy-start | bytes 388
  196.7 5.4 %copy-start.18 = (f32[64,2]{0,1:T(2,128)S(1)}, f32[64,2]{0,1:T(2,128)}, u32[]{:S(2)}) copy-start(f32[64,2]{0,1:T(2,128)} %param.33) | copy-start | bytes 1540
  196.7 5.5 %copy-start.14 = (s32[128]{0:T(128)S(1)}, s32[128]{0:T(128)}, u32[]{:S(2)}) copy-start(s32[128]{0:T(128)} %copy-done.13) | copy-start | bytes 1540
  196.7 46.7 %reduce-scatter.7.cloned.1.call-start = ((), (), s32[]{:S(2)}) async-start(), calls=%async_computation.6 | async-start | bytes 1310720 | tf_op jit(solution)/shard_map/reduce_scatter | solution.py:229
  196.8 3.5 %copy-start.5 = (bf16[128,2048]{1,0:T(8,128)(2,1)S(1)}, bf16[128,2048]{1,0:T(8,128)(2,1)}, u32[]{:S(2)}) copy-start(bf16[128,2048]{1,0:T(8,128)(2,1)} %param.29) | copy-start | bytes 1572868
  (2 other events, 1.1 us)
Sparse Core Ops, SparseCore 0:
  47.5 33.5 all-gather.6
  83.2 16.6 all-gather.8
  102.0 40.7 all-gather.4
  145.2 43.1 reduce-scatter.10
  190.8 24.8 reduce-scatter.8
  218.6 24.7 reduce-scatter.6
where the time goes:
time: 251 us; the launch traced here: 250 us
  waiting for transfers between devices  87.2 us (35%)
  blocking collectives  80.8 us (32%)
  matrix products  32 us (13%)
  local copies, waits for them, and re-layouts  19.8 us (8%)
  between operations  14.6 us (6%)
  other arithmetic  10.1 us (4%)
  starting transfers between devices  5.76 us (2%)
    all_to_all x1, blocking collectives, shards(): lax.all_to_all(outgoing, 'ep', split_axis=0, concat_axis=0, tiled=True)  32.8 us
    all_gather x1, blocking collectives, shards(): lax.all_gather(group_turn, 'ep', axis=0, tiled=True)  31.1 us
    all_gather x1, waiting for transfers between devices, shards(): lax.all_gather(received, 'tp', axis=0, tiled=True)  26.7 us
    unnamed x7, waiting for transfers between devices  26.6 us
    all_to_all x1, waiting for transfers between devices, shards(): lax.all_to_all(routed_sum.astype(jnp.bfloat16), 'ep', split_axis=0, conca...  20.1 us
    unnamed x44, local copies, waits for them, and re-layouts  14.2 us
    reduce_scatter x1, waiting for transfers between devices, shards(): lax.psum_scatter(mixer_term.astype(jnp.bfloat16), 'tp', scatter_dimension...  13.7 us
    dot_general x1, matrix products, expert_terms(): jnp.einsum('secf,efd->secd', hidden, down_weight, preferred_element_type=...  7.31 us
  transfers between devices with their start and end apart: 7, of which 4 were waited for; matrix products, arithmetic and copies ran while one was open for 21% of the time, Pallas kernels for 0%

commit v1 on v0

--- a/solution.py
+++ b/solution.py
@@ -3,6 +3,8 @@
 import jax
 import jax.numpy as jnp
 from jax import lax
+from jax.experimental import pallas as pl
+from jax.experimental.pallas import tpu as pltpu
 from jax.sharding import PartitionSpec as P
 
 HEADS = 8
@@ -106,7 +108,7 @@
     return jnp.dot(hidden, down_weight, preferred_element_type=jnp.float32)
 
 
-def shards(
+def shards_plain(
     query_latent,
     key_latent,
     rotary_key,
@@ -247,6 +249,578 @@
     return (mixer_out, expert_out)
 
 
+MESH = pl.DeviceIdType.MESH
+VMEM_LIMIT = 60 * 1024 * 1024
+
+
+def greet(ep_count, me, head_index):
+    barrier = pltpu.get_barrier_semaphore()
+    for step in range(1, ep_count):
+        pl.semaphore_signal(
+            barrier, inc=1, device_id=(lax.rem(me + step, ep_count), head_index), device_id_type=MESH
+        )
+    row, core = head_index // 2, head_index % 2
+    for other in ((1 - row) * 2 + core, row * 2 + 1 - core):
+        pl.semaphore_signal(barrier, inc=1, device_id=(me, other), device_id_type=MESH)
+    pl.semaphore_wait(barrier, ep_count + 1)
+
+
+def spread_kernel(
+    ep_count,
+    slots_ref,
+    latent_ref,
+    tokens_ref,
+    query_ref,
+    rows_out,
+    latent_out,
+    tokens_out,
+    query_out,
+    ep_send,
+    ep_recv,
+    y_send,
+    y_recv,
+    core_send,
+    core_recv,
+    cross_send,
+    cross_recv,
+    own_sem,
+):
+    me = lax.axis_index("ep")
+    head_index = lax.axis_index("tp")
+    row, core = head_index // 2, head_index % 2
+    y_peer = (me, (1 - row) * 2 + core)
+    core_peer = (me, row * 2 + 1 - core)
+    greet(ep_count, me, head_index)
+
+    def remote(source, target, send_sem, recv_sem, device):
+        return pltpu.make_async_remote_copy(
+            src_ref=source,
+            dst_ref=target,
+            send_sem=send_sem,
+            recv_sem=recv_sem,
+            device_id=device,
+            device_id_type=MESH,
+        )
+
+    def ep_copies(step):
+        peer = lax.rem(me + step, ep_count)
+        return (
+            remote(
+                latent_ref,
+                latent_out.at[row, core, me],
+                ep_send.at[1, step],
+                ep_recv.at[1, step],
+                (peer, head_index),
+            ),
+            remote(
+                slots_ref.at[peer],
+                rows_out.at[row, core, me],
+                ep_send.at[0, step],
+                ep_recv.at[0, step],
+                (peer, head_index),
+            ),
+        )
+
+    def block_copies(origin_row, step, send_sem, recv_sem, device):
+        origin = lax.rem(me + ep_count - step, ep_count)
+        return (
+            remote(
+                latent_out.at[origin_row, core, origin],
+                latent_out.at[origin_row, core, origin],
+                send_sem.at[1, step],
+                recv_sem.at[1, step],
+                device,
+            ),
+            remote(
+                rows_out.at[origin_row, core, origin],
+                rows_out.at[origin_row, core, origin],
+                send_sem.at[0, step],
+                recv_sem.at[0, step],
+                device,
+            ),
+        )
+
+    def group_copies(origin_row, send_sem, recv_sem, device):
+        return (
+            remote(
+                tokens_out.at[origin_row, core],
+                tokens_out.at[origin_row, core],
+                send_sem.at[0, ep_count],
+                recv_sem.at[0, ep_count],
+                device,
+            ),
+            remote(
+                query_out.at[origin_row, core],
+                query_out.at[origin_row, core],
+                send_sem.at[1, ep_count],
+                recv_sem.at[1, ep_count],
+                device,
+            ),
+        )
+
+    own = (
+        pltpu.make_async_copy(latent_ref, latent_out.at[row, core, me], own_sem.at[0]),
+        pltpu.make_async_copy(slots_ref.at[me], rows_out.at[row, core, me], own_sem.at[1]),
+        pltpu.make_async_copy(tokens_ref, tokens_out.at[row, core], own_sem.at[2]),
+        pltpu.make_async_copy(query_ref, query_out.at[row, core], own_sem.at[3]),
+    )
+    for copy in own:
+        copy.start()
+    for step in range(1, ep_count):
+        for copy in ep_copies(step):
+            copy.start()
+    for copy in own:
+        copy.wait()
+    own_row, far_row = row, 1 - row
+    for copy in group_copies(own_row, y_send, y_recv, y_peer):
+        copy.start()
+    for copy in group_copies(own_row, core_send, core_recv, core_peer):
+        copy.start()
+    for step in range(ep_count + 1):
+        if step < ep_count:
+            if step > 0:
+                for copy in ep_copies(step):
+                    copy.wait_recv()
+            for copy in block_copies(own_row, step, y_send, y_recv, y_peer):
+                copy.start()
+            for copy in block_copies(own_row, step, core_send, core_recv, core_peer):
+                copy.start()
+        if step == 0:
+            for copy in group_copies(own_row, y_send, y_recv, y_peer):
+                copy.wait_recv()
+            for copy in group_copies(far_row, cross_send, cross_recv, core_peer):
+                copy.start()
+        else:
+            for copy in block_copies(own_row, step - 1, y_send, y_recv, y_peer):
+                copy.wait_recv()
+            for copy in block_copies(far_row, step - 1, cross_send, cross_recv, core_peer):
+                copy.start()
+    for step in range(1, ep_count):
+        for copy in ep_copies(step):
+            copy.wait_send()
+    waits = [
+        (own_row, y_send, y_recv, y_peer, False),
+        (own_row, core_send, core_recv, core_peer, True),
+        (far_row, cross_send, cross_recv, core_peer, True),
+    ]
+    for origin_row, send_sem, recv_sem, device, both in waits:
+        for copy in group_copies(origin_row, send_sem, recv_sem, device):
+            copy.wait_send()
+            if both:
+                copy.wait_recv()
+        for step in range(ep_count):
+            for copy in block_copies(origin_row, step, send_sem, recv_sem, device):
+                copy.wait_send()
+                if both:
+                    copy.wait_recv()
+
+
+def spread(slots, latent_pack, tokens, queries):
+    ep_count, row_count, width = slots.shape
+    vmem = pl.BlockSpec(memory_space=pltpu.VMEM)
+    semaphores = pltpu.SemaphoreType.DMA((2, ep_count + 1))
+    return pl.pallas_call(
+        lambda *refs: spread_kernel(ep_count, *refs),
+        out_shape=(
+            jax.ShapeDtypeStruct((2, 2, ep_count, row_count, width), jnp.bfloat16),
+            jax.ShapeDtypeStruct((2, 2, ep_count) + latent_pack.shape, jnp.bfloat16),
+            jax.ShapeDtypeStruct((2, 2) + tokens.shape, jnp.bfloat16),
+            jax.ShapeDtypeStruct((2, 2) + queries.shape, jnp.bfloat16),
+        ),
+        in_specs=[vmem] * 4,
+        out_specs=(vmem,) * 4,
+        scratch_shapes=[semaphores] * 8 + [pltpu.SemaphoreType.DMA((4,))],
+        compiler_params=pltpu.CompilerParams(
+            collective_id=0, has_side_effects=True, vmem_limit_bytes=VMEM_LIMIT
+        ),
+        name="spread",
+    )(slots, latent_pack, tokens, queries)
+
+
+def gated_rows(rows, gate_weight, up_weight):
+    gated = jnp.dot(rows, gate_weight, preferred_element_type=jnp.float32)
+    lifted = jnp.dot(rows, up_weight, preferred_element_type=jnp.float32)
+    return (gated / (1.0 + jnp.exp(-gated)) * lifted).astype(jnp.bfloat16)
+
+
+def finish_kernel(
+    ep_count,
+    capacity,
+    rows_ref,
+    tokens_ref,
+    mixer_ref,
+    gate_ref,
+    up_ref,
+    down_ref,
+    shared_gate_ref,
+    shared_up_ref,
+    shared_down_ref,
+    weight_ref,
+    mixer_out,
+    expert_out,
+    part,
+    side,
+    half_rows,
+    half_side,
+    far_rows,
+    far_side,
+    returned,
+    core_send,
+    core_recv,
+    y_send,
+    y_recv,
+    ep_send,
+    ep_recv,
+):
+    me = lax.axis_index("ep")
+    head_index = lax.axis_index("tp")
+    row, core = head_index // 2, head_index % 2
+    y_peer = (me, (1 - row) * 2 + core)
+    core_peer = (me, row * 2 + 1 - core)
+    greet(ep_count, me, head_index)
+    local_experts = gate_ref.shape[0]
+    width = rows_ref.shape[-1]
+    own_rows = tokens_ref.shape[2]
+    slot_rows = rows_ref.shape[3]
+    stripe = math.gcd(width, 512)
+
+    def remote(source, target, send_sem, recv_sem, device):
+        return pltpu.make_async_remote_copy(
+            src_ref=source,
+            dst_ref=target,
+            send_sem=send_sem,
+            recv_sem=recv_sem,
+            device_id=device,
+            device_id_type=MESH,
+        )
+
+    def compute(side_core):
+        for expert in range(local_experts):
+            span = slice(expert * capacity, (expert + 1) * capacity)
+            block = rows_ref[:, side_core, :, span, :].reshape(2 * ep_count * capacity, width)
+            hidden = gated_rows(block, gate_ref[expert], up_ref[expert])
+            for start in range(0, width, stripe):
+                product = jnp.dot(
+                    hidden,
+                    down_ref[expert, :, start : start + stripe],
+                    preferred_element_type=jnp.float32,
+                ).astype(jnp.bfloat16)
+                part[:, side_core, :, span, start : start + stripe] = product.reshape(
+                    2, ep_count, capacity, stripe
+                )
+        block = tokens_ref[:, side_core].reshape(2 * own_rows, width)
+        hidden = gated_rows(block, shared_gate_ref[...], shared_up_ref[...])
+        for start in range(0, width, stripe):
+            product = jnp.dot(
+                hidden,
+                shared_down_ref[:, start : start + stripe],
+                preferred_element_type=jnp.float32,
+            ).astype(jnp.bfloat16)
+            side[:, side_core, :own_rows, start : start + stripe] = product.reshape(
+                2, own_rows, stripe
+            )
+        side[:, side_core, own_rows:, :] = mixer_ref[:, side_core]
+
+    def core_copies(target_row, place):
+        return (
+            remote(
+                part.at[target_row, 1 - core],
+                half_rows.at[target_row],
+                core_send.at[place, 0],
+                core_recv.at[place, 0],
+                core_peer,
+            ),
+            remote(
+                side.at[target_row, 1 - core],
+                half_side.at[target_row],
+                core_send.at[place, 1],
+                core_recv.at[place, 1],
+                core_peer,
+            ),
+        )
+
+    compute(1 - core)
+    near, far = core_copies(row, 0), core_copies(1 - row, 1)
+    for copy in far + near:
+        copy.start()
+    compute(core)
+
+    def y_copy(block):
+        return remote(
+            part.at[1 - row, core, block],
+            far_rows.at[block],
+            y_send.at[block],
+            y_recv.at[block],
+            y_peer,
+        )
+
+    def ep_copy(step):
+        peer = lax.rem(me + step, ep_count)
+        return remote(
+            part.at[row, core, peer],
+            returned.at[me],
+            ep_send.at[step],
+            ep_recv.at[step],
+            (peer, head_index),
+        )
+
+    side_copy = remote(
+        side.at[1 - row, core], far_side, y_send.at[ep_count], y_recv.at[ep_count], y_peer
+    )
+    far[0].wait_recv()
+    for step in range(ep_count):
+        block = lax.rem(me + step + 1, ep_count)
+        part[1 - row, core, block] = (
+            part[1 - row, core, block].astype(jnp.float32)
+            + half_rows[1 - row, block].astype(jnp.float32)
+        ).astype(jnp.bfloat16)
+        y_copy(block).start()
+    far[1].wait_recv()
+    side[1 - row, core] = (
+        side[1 - row, core].astype(jnp.float32) + half_side[1 - row].astype(jnp.float32)
+    ).astype(jnp.bfloat16)
+    side_copy.start()
+    near[0].wait_recv()
+    for step in range(ep_count):
+        block = lax.rem(me + step + 1, ep_count)
+        y_copy(block).wait_recv()
+        total = (
+            part[row, core, block].astype(jnp.float32)
+            + half_rows[row, block].astype(jnp.float32)
+            + far_rows[block].astype(jnp.float32)
+        ).astype(jnp.bfloat16)
+        if step + 1 < ep_count:
+            part[row, core, block] = total
+            ep_copy(step + 1).start()
+        else:
+            returned[me] = total
+    near[1].wait_recv()
+    side_copy.wait_recv()
+    side_total = (
+        side[row, core].astype(jnp.float32)
+        + half_side[row].astype(jnp.float32)
+        + far_side[...].astype(jnp.float32)
+    )
+    mixer_out[...] = side_total[own_rows:].astype(jnp.bfloat16)
+    for step in range(1, ep_count):
+        ep_copy(step).wait_recv()
+    for start in range(0, width, stripe):
+        picked = jnp.dot(
+            weight_ref[...],
+            returned[:, :, start : start + stripe].reshape(ep_count * slot_rows, stripe),
+            preferred_element_type=jnp.float32,
+        )
+        picked = picked[:own_rows] + picked[own_rows : 2 * own_rows] + picked[2 * own_rows :]
+        expert_out[:, start : start + stripe] = (
+            picked + side_total[:own_rows, start : start + stripe]
+        ).astype(jnp.bfloat16)
+    for copy in far + near:
+        copy.wait_send()
+    for block in range(ep_count):
+        y_copy(block).wait_send()
+    side_copy.wait_send()
+    for step in range(1, ep_count):
+        ep_copy(step).wait_send()
+
+
+def finish(capacity, *operands):
+    rows, tokens = operands[0], operands[1]
+    ep_count, slot_rows, width = rows.shape[2:]
+    own_rows = tokens.shape[2]
+    vmem = pl.BlockSpec(memory_space=pltpu.VMEM)
+    out = jax.ShapeDtypeStruct((own_rows, width), jnp.bfloat16)
+    return pl.pallas_call(
+        lambda *refs: finish_kernel(ep_count, capacity, *refs),
+        out_shape=(out, out),
+        in_specs=[vmem] * len(operands),
+        out_specs=(vmem, vmem),
+        scratch_shapes=[
+            pltpu.VMEM(rows.shape, jnp.bfloat16),
+            pltpu.VMEM((2, 2, 2 * own_rows, width), jnp.bfloat16),
+            pltpu.VMEM((2, ep_count, slot_rows, width), jnp.bfloat16),
+            pltpu.VMEM((2, 2 * own_rows, width), jnp.bfloat16),
+            pltpu.VMEM((ep_count, slot_rows, width), jnp.bfloat16),
+            pltpu.VMEM((2 * own_rows, width), jnp.bfloat16),
+            pltpu.VMEM((ep_count, slot_rows, width), jnp.bfloat16),
+            pltpu.SemaphoreType.DMA((2, 2)),
+            pltpu.SemaphoreType.DMA((2, 2)),
+            pltpu.SemaphoreType.DMA((ep_count + 1,)),
+            pltpu.SemaphoreType.DMA((ep_count + 1,)),
+            pltpu.SemaphoreType.DMA((ep_count,)),
+            pltpu.SemaphoreType.DMA((ep_count,)),
+        ],
+        compiler_params=pltpu.CompilerParams(
+            collective_id=1, has_side_effects=True, vmem_limit_bytes=VMEM_LIMIT
+        ),
+        name="finish",
+    )(*operands)
+
+
+def shards(
+    query_latent,
+    key_latent,
+    rotary_key,
+    query_gain,
+    latent_gain,
+    query_content,
+    query_rotary,
+    key_content,
+    value_weight,
+    output_weight,
+    expert_input,
+    norm_gain,
+    routes,
+    route_weight,
+    expert_gate,
+    expert_up,
+    expert_down,
+    shared_gate,
+    shared_up,
+    shared_down,
+):
+    group_size = lax.axis_size("tp")
+    expert_groups = lax.axis_size("ep")
+    token_rows = expert_input.shape[0]
+    picks = routes.shape[1]
+    local_experts = expert_gate.shape[0]
+    expert_total = local_experts * expert_groups
+    capacity = 2 * token_rows * picks // expert_total
+    if group_size != 4 or capacity % 16:
+        return shards_plain(
+            query_latent,
+            key_latent,
+            rotary_key,
+            query_gain,
+            latent_gain,
+            query_content,
+            query_rotary,
+            key_content,
+            value_weight,
+            output_weight,
+            expert_input,
+            norm_gain,
+            routes,
+            route_weight,
+            expert_gate,
+            expert_up,
+            expert_down,
+            shared_gate,
+            shared_up,
+            shared_down,
+        )
+    own_rows = query_latent.shape[0]
+    head_local = HEADS // group_size
+    head_index = lax.axis_index("tp")
+    group_rows_count = own_rows * group_size
+    group_start = lax.axis_index("ep") * group_rows_count
+    own_start = group_start + head_index * own_rows
+    score_scale = (CONTENT + ROTARY) ** (-0.5)
+    query_normed = rms_rows(query_latent, query_gain).astype(jnp.bfloat16)
+    latent_normed = rms_rows(key_latent, latent_gain).astype(jnp.bfloat16)
+    own_positions = own_start + jnp.arange(own_rows, dtype=jnp.int32)
+    key_turned = turn_pairs(rotary_key.astype(jnp.float32)[:, None, :], own_positions)[
+        :, 0, :
+    ].astype(jnp.bfloat16)
+    slot_total = expert_total * capacity
+    model_width = expert_input.shape[1]
+    expert_normed = rms_rows(expert_input, norm_gain).astype(jnp.bfloat16)
+    flat_routes = routes.reshape(-1)
+    marks = (flat_routes[:, None] == jnp.arange(expert_total, dtype=jnp.int32)[None, :]).astype(
+        jnp.int32
+    )
+    ranks = jnp.sum((jnp.cumsum(marks, 0) - marks) * marks, 1)
+    targets = (flat_routes * capacity + ranks).reshape(token_rows, picks)
+    chosen = targets[:, :, None] == jnp.arange(slot_total, dtype=jnp.int32)[None, None, :]
+    picker = jnp.any(chosen, 1).astype(jnp.bfloat16)
+    spread_weight = jnp.sum(jnp.where(chosen, route_weight[:, :, None], 0.0), 1)
+    high = lax.reduce_precision(spread_weight, 8, 7)
+    middle = lax.reduce_precision(spread_weight - high, 8, 7)
+    low = spread_weight - high - middle
+    weight_terms = jnp.concatenate([high, middle, low], 0).astype(jnp.bfloat16)
+    slots = lax.dot_general(
+        picker, expert_normed, (((0,), (0,)), ((), ())), preferred_element_type=jnp.float32
+    ).astype(jnp.bfloat16)
+    slots = slots.reshape(expert_groups, local_experts * capacity, model_width)
+    rank_width = latent_normed.shape[1]
+    pad_width = -rotary_key.shape[1] % 128
+    latent_pack = jnp.concatenate(
+        [latent_normed, key_turned, jnp.zeros((own_rows, pad_width), jnp.bfloat16)], 1
+    )
+    gathered_rows, packs, gathered_tokens, group_query = spread(
+        slots, latent_pack, expert_normed, query_normed
+    )
+    packs = (
+        packs.reshape(group_size, expert_groups, own_rows, -1)
+        .transpose(1, 0, 2, 3)
+        .reshape(expert_groups * group_rows_count, -1)
+    )
+    group_query = group_query.reshape(group_rows_count, -1)
+    positions = group_start + jnp.arange(group_rows_count, dtype=jnp.int32)
+    content_columns = lax.dynamic_slice_in_dim(
+        query_content, head_index * head_local * CONTENT, head_local * CONTENT, 1
+    )
+    rotary_columns = lax.dynamic_slice_in_dim(
+        query_rotary, head_index * head_local * ROTARY, head_local * ROTARY, 1
+    )
+    query_part = (
+        jnp.dot(group_query, content_columns, preferred_element_type=jnp.float32)
+        .astype(jnp.bfloat16)
+        .reshape(group_rows_count, head_local, CONTENT)
+    )
+    query_turn = turn_pairs(
+        jnp.dot(group_query, rotary_columns, preferred_element_type=jnp.float32).reshape(
+            group_rows_count, head_local, ROTARY
+        ),
+        positions,
+    ).astype(jnp.bfloat16)
+    key_columns = lax.dynamic_slice_in_dim(
+        key_content, head_index * head_local * CONTENT, head_local * CONTENT, 1
+    )
+    value_columns = lax.dynamic_slice_in_dim(
+        value_weight, head_index * head_local * VALUE, head_local * VALUE, 1
+    )
+    carry_start = (
+        jnp.full((group_rows_count, head_local), -jnp.inf, jnp.float32),
+        jnp.zeros((group_rows_count, head_local), jnp.float32),
+        jnp.zeros((group_rows_count, head_local, VALUE), jnp.float32),
+    )
+    key_part, value_rows = expand_keys(
+        packs[:, :rank_width], key_columns, value_columns, head_local
+    )
+    running_peak, running_total, summed = absorb_piece(
+        carry_start,
+        query_part,
+        query_turn,
+        key_part,
+        packs[:, rank_width : rank_width + rotary_key.shape[1]],
+        value_rows,
+        score_scale,
+    )
+    attended = (
+        (summed / running_total[..., None])
+        .astype(jnp.bfloat16)
+        .reshape(group_rows_count, head_local * VALUE)
+    )
+    mixer_term = (
+        jnp.dot(attended, output_weight, preferred_element_type=jnp.float32)
+        .astype(jnp.bfloat16)
+        .reshape(2, 2, own_rows, model_width)
+    )
+    return finish(
+        capacity,
+        gathered_rows,
+        gathered_tokens,
+        mixer_term,
+        expert_gate,
+        expert_up,
+        expert_down,
+        shared_gate,
+        shared_up,
+        shared_down,
+        weight_terms,
+    )
+
+
 def solution(mesh):
     in_specs = (
         P(("ep", "tp"), None),

time: 251 us -> 145 us (0.58)
  Pallas kernels: 0 us -> 112 us
  waiting for transfers between devices: 87.2 us -> 0 us
  blocking collectives: 80.8 us -> 0 us
  matrix products: 32 us -> 14.2 us
  between operations: 14.6 us -> 0.95 us
  local copies, waits for them, and re-layouts: 19.8 us -> 6.61 us
  starting transfers between devices: 5.76 us -> 0 us
    pallas_call x0 -> x2, Pallas kernels: none -> 112 us  [the longest x1 57.1 us: finish(): pl.pallas_call(lambda *refs: finish_kernel(ep_count, capacity, *refs), ou...]
    all_gather x4 -> x0, blocking collectives: 47.9 us -> none  [the longest x1 31.1 us: shards(): lax.all_gather(group_turn, 'ep', axis=0, tiled=True)]
    all_to_all x1 -> x0, blocking collectives: 32.8 us -> none  [shards(): lax.all_to_all(outgoing, 'ep', split_axis=0, concat_axis=0, tiled=True)]
    all_gather x3 -> x0, waiting for transfers between devices: 26.7 us -> none  [the longest x1 26.7 us: shards(): lax.all_gather(received, 'tp', axis=0, tiled=True)]
    unnamed x7 -> x0, waiting for transfers between devices: 26.6 us -> none
    all_to_all x1 -> x0, waiting for transfers between devices: 20.1 us -> none  [shards(): lax.all_to_all(routed_sum.astype(jnp.bfloat16), 'ep', split_axis=0, conca...]
    dot_general x5 -> x1, matrix products: 18.8 us -> 1.47 us  [shards(): lax.dot_general(picker, expert_normed, (((0,), (0,)), ((), ())), preferre...]
    reduce_scatter x2 -> x0, waiting for transfers between devices: 13.7 us -> none  [the longest x1 13.7 us: shards(): lax.psum_scatter(mixer_term.astype(jnp.bfloat16), 'tp', scatter_dimension...]
  transfers between devices with their start and end apart: 7 -> 0, of which waited for: 4 -> 0; matrix products, arithmetic and copies ran while one was open for 21% -> 0% of each run, Pallas kernels for 0% -> 0%
where the time goes in v1:
time: 145 us; the launch traced here: 144 us
  Pallas kernels  112 us (77%)
  matrix products  14.2 us (10%)
  other arithmetic  10.7 us (7%)
  local copies, waits for them, and re-layouts  6.61 us (5%)
    pallas_call x1, Pallas kernels, finish(): pl.pallas_call(lambda *refs: finish_kernel(ep_count, capacity, *refs), ou...  57.1 us
    pallas_call x1, Pallas kernels, spread(): pl.pallas_call(lambda *refs: spread_kernel(ep_count, *refs), out_shape=(j...  54.7 us
    unnamed x13, local copies, waits for them, and re-layouts  4.14 us
    dot_general x1, matrix products, absorb_block(): jnp.einsum('qhc,khc->qhk', query_part, key_part, preferred_element_type=j...  2.98 us
    reduce_sum x3, other arithmetic, rms_rows(): jnp.mean(widened * widened, -1, keepdims=True) + norm_eps  2.93 us

profile of v1, /device:TPU:0, one launch (start us, length us, event | category | flops | bytes accessed | tf_op | source)
XLA Modules:
  0.0 144.3 jit_solution(17938829554342884751)
XLA Ops:
  0.7 0.8 bitcast_convert_fusion
  1.7 0.9 fusion.29
  2.6 0.8 fusion.31
  4.2 0.8 copy.57
  5.8 0.7 multiply_add_fusion
  6.6 1.1 fusion.20
  7.7 1.1 fusion.22.refs_2_
  8.8 1.5 %convolution_convert_fusion.1 = bf16[256,2048]{1,0:T(8,128)(2,1)} fusion(pred[64,256]{1,0:T(8,128)(4,1)S(1)} %fusion.28, bf16[64,2048]{1,0:T(8,128)(2,1)S(1)} %fusion.22.refs_2_), kind=kOutput, calls=%fused_computation.6 | convolution fusion | flops 67633152 | bytes 1327104 | tf_op jit(solution)/shard_map/dot_general | solution.py:740
  10.3 1.0 fusion.24
  11.2 1.6 %fusion.26.refs_3_ = bf16[64,512]{1,0:T(8,128)(2,1)} fusion(bf16[64,512]{1,0:T(8,128)(2,1)} %param.20, f32[512]{0:T(512)} %param.23, f32[64]{0:T(128)S(1)} %add_rsqrt_fusion), kind=kLoop, calls=%fused_computation.29 | loop fusion | flops 131072 | bytes 133376 | tf_op jit(solution)/shard_map/convert_element_type | solution.py:718
  12.8 54.7 %spread.1 = (bf16[2,2,8,32,2048]{4,3,2,1,0:T(8,128)(2,1)}, bf16[2,2,8,64,384]{4,3,2,1,0:T(8,128)(2,1)}, bf16[2,2,64,2048]{3,2,1,0:T(8,128)(2,1)}, bf16[2,2,64,512]{3,2,1,0:T(8,128)(2,1)}) custom-call(bf16[8,32,2048]{2,1,0:T(8,128)(2,1)} %bitcast.58, bf16[64,384]{1,0:T(8,128)(2,1)} %maximum_maximum_fusion.refs_1_, bf16[64,2048]{1,0:T(8,128)(2,1)} %copy-done.1, ...), custom_call_target="tpu_custom_call" | custom-call | tf_op jit(solution)/shard_map/spread/pallas_call | solution.py:422
  67.7 1.2 fusion.54
  69.1 1.6 %copy.61 = bf16[4,8,64,384]{3,2,0,1:T(8,128)(2,1)S(1)} copy(bf16[4,8,64,384]{3,2,1,0:T(8,128)(2,1)} %bitcast.62) | data formatting | bytes 3145728 | tf_op jit(solution)/shard_map/reshape | solution.py:753
  70.8 2.7 %fusion.23 = f32[256,2,2048]{0,2,1:T(8,128)} fusion(bf16[2048,384]{1,0:T(8,128)(2,1)S(1)} %bitcast.55, bf16[256,2,32]{0,1,2:T(2,128)(2,1)S(1)} %bitcast.68), kind=kOutput, calls=%fused_computation.24 | convolution fusion | flops 67108864 | bytes 4751360 | tf_op jit(solution)/shard_map/qhr,kr->qhk/dot_general | solution.py:42
  73.4 1.3 convolution_convert_fusion.3
  74.8 1.1 convolution_convert_fusion.4
  75.9 3.0 %fusion.53 = (f32[256,2]{0,1:T(2,128)S(1)}, f32[256,2,2048]{0,2,1:T(8,128)S(1)}) fusion(f32[256,2,2048]{0,2,1:T(8,128)} %fusion.23, bf16[2048,2,64]{0,2,1:T(8,128)(2,1)S(1)} %bitcast.61, bf16[256,2,64]{0,2,1:T(8,128)(2,1)S(1)} %bitcast.66), kind=kOutput, calls=%fused_computation.86 | convolution fusion | flops 137362944 | bytes 8980480 | tf_op jit(solution)/shard_map/qhc,khc->qhk/dot_general | solution.py:41
  79.5 1.3 convolution_convert_fusion.2
  80.8 0.8 fusion.15
  81.6 1.4 convolution_convert_fusion
  83.2 0.6 pad_maximum_fusion.refs_9_
  83.8 57.1 %finish.1 = (bf16[64,2048]{1,0:T(8,128)(2,1)}, bf16[64,2048]{1,0:T(8,128)(2,1)}) custom-call(bf16[2,2,8,32,2048]{4,3,2,1,0:T(8,128)(2,1)} %get-tuple-element.6.refs_0_, bf16[2,2,64,2048]{3,2,1,0:T(8,128)(2,1)} %get-tuple-element.7.refs_1_, bf16[2,2,64,2048]{3,2,1,0:T(8,128)(2,1)} %bitcast.59, bf16[2,2048,256]{2,1,0:T(8,128)(2,1)} %refs_3_.1, ...), custom_call_target="tpu_custom_call" | custom-call | tf_op jit(solution)/shard_map/finish/pallas_call | solution.py:632
  140.9 1.7 %copy.75 = bf16[64,2048]{1,0:T(8,128)(2,1)} copy(bf16[64,2048]{1,0:T(8,128)(2,1)} %get-tuple-element.25) | data formatting | bytes 524288
  142.6 1.7 %copy.76 = bf16[64,2048]{1,0:T(8,128)(2,1)} copy(bf16[64,2048]{1,0:T(8,128)(2,1)} %get-tuple-element.26) | data formatting | bytes 524288
  (44 shorter events, 3.0 us)
Async XLA Ops:
  0.6 81.0 %copy-start = (bf16[128,2048]{1,0:T(8,128)(2,1)S(1)}, bf16[128,2048]{1,0:T(8,128)(2,1)}, u32[]{:S(2)}) copy-start(bf16[128,2048]{1,0:T(8,128)(2,1)} %param.29) | copy-start | bytes 1572868
  0.6 66.8 %copy-start.3 = (bf16[512,256]{1,0:T(8,128)(2,1)S(1)}, bf16[512,256]{1,0:T(8,128)(2,1)}, u32[]{:S(2)}) copy-start(bf16[512,256]{1,0:T(8,128)(2,1)} %param.26) | copy-start | bytes 786436
  8.8 4.0 %copy-start.1 = (bf16[64,2048]{1,0:T(8,128)(2,1)}, bf16[64,2048]{1,0:T(8,128)(2,1)S(1)}, u32[]{:S(2)}) copy-start(bf16[64,2048]{1,0:T(8,128)(2,1)S(1)} %fusion.22.refs_2_) | copy-start | bytes 786436
  69.1 5.6 %copy-start.2 = (bf16[2,2,64,512]{3,2,1,0:T(8,128)(2,1)S(1)}, bf16[2,2,64,512]{3,2,1,0:T(8,128)(2,1)}, u32[]{:S(2)}) copy-start(bf16[2,2,64,512]{3,2,1,0:T(8,128)(2,1)} %get-tuple-element.9) | copy-start | bytes 786436
  79.5 3.6 %copy-start.4 = (f32[64,2]{0,1:T(2,128)S(1)}, f32[64,2]{0,1:T(2,128)}, u32[]{:S(2)}) copy-start(f32[64,2]{0,1:T(2,128)} %param.33) | copy-start | bytes 1540

commit v2 on v0

--- a/solution.py
+++ b/solution.py
@@ -3,6 +3,8 @@
 import jax
 import jax.numpy as jnp
 from jax import lax
+from jax.experimental import pallas as pl
+from jax.experimental.pallas import tpu as pltpu
 from jax.sharding import PartitionSpec as P
 
 HEADS = 8
@@ -106,7 +108,7 @@
     return jnp.dot(hidden, down_weight, preferred_element_type=jnp.float32)
 
 
-def shards(
+def shards_plain(
     query_latent,
     key_latent,
     rotary_key,
@@ -247,6 +249,623 @@
     return (mixer_out, expert_out)
 
 
+MESH = pl.DeviceIdType.MESH
+VMEM_LIMIT = 60 * 1024 * 1024
+
+
+def greet(ep_count, me, head_index):
+    barrier = pltpu.get_barrier_semaphore()
+    for step in range(1, ep_count):
+        pl.semaphore_signal(
+            barrier, inc=1, device_id=(lax.rem(me + step, ep_count), head_index), device_id_type=MESH
+        )
+    row, core = head_index // 2, head_index % 2
+    for other in ((1 - row) * 2 + core, row * 2 + 1 - core):
+        pl.semaphore_signal(barrier, inc=1, device_id=(me, other), device_id_type=MESH)
+    pl.semaphore_wait(barrier, ep_count + 1)
+
+
+def gated_rows(rows, gate_weight, up_weight):
+    gated = jnp.dot(rows, gate_weight, preferred_element_type=jnp.float32)
+    lifted = jnp.dot(rows, up_weight, preferred_element_type=jnp.float32)
+    return (gated / (1.0 + jnp.exp(-gated)) * lifted).astype(jnp.bfloat16)
+
+
+def block_kernel(
+    ep_count,
+    capacity,
+    slots_ref,
+    latent_ref,
+    tokens_ref,
+    query_ref,
+    query_columns_ref,
+    latent_columns_ref,
+    turns_ref,
+    output_weight_ref,
+    weight_ref,
+    gate_hbm,
+    up_hbm,
+    down_hbm,
+    shared_gate_hbm,
+    shared_up_hbm,
+    shared_down_hbm,
+    mixer_out,
+    expert_out,
+    rows,
+    latents,
+    tokens,
+    queries,
+    gate_ref,
+    up_ref,
+    down_ref,
+    shared_gate_ref,
+    shared_up_ref,
+    shared_down_ref,
+    keys,
+    values,
+    query_wide,
+    attended,
+    part,
+    side,
+    half_rows,
+    half_side,
+    far_rows,
+    far_side,
+    returned,
+    ep_send,
+    ep_recv,
+    y_send,
+    y_recv,
+    core_send,
+    core_recv,
+    cross_send,
+    cross_recv,
+    own_sem,
+    weight_sem,
+    half_send,
+    half_recv,
+    far_send,
+    far_recv,
+    back_send,
+    back_recv,
+):
+    me = lax.axis_index("ep")
+    head_index = lax.axis_index("tp")
+    row, core = head_index // 2, head_index % 2
+    y_peer = (me, (1 - row) * 2 + core)
+    core_peer = (me, row * 2 + 1 - core)
+    local_experts = gate_ref.shape[0]
+    width = rows.shape[-1]
+    own_rows = tokens.shape[2]
+    slot_rows = rows.shape[3]
+    stripe = math.gcd(width, 512)
+
+    def remote(source, target, send_sem, recv_sem, device):
+        return pltpu.make_async_remote_copy(
+            src_ref=source,
+            dst_ref=target,
+            send_sem=send_sem,
+            recv_sem=recv_sem,
+            device_id=device,
+            device_id_type=MESH,
+        )
+
+    fetches = [
+        pltpu.make_async_copy(source, target, weight_sem.at[place])
+        for place, (source, target) in enumerate(
+            (
+                (shared_gate_hbm, shared_gate_ref),
+                (shared_up_hbm, shared_up_ref),
+                (shared_down_hbm, shared_down_ref),
+                (gate_hbm, gate_ref),
+                (up_hbm, up_ref),
+                (down_hbm, down_ref),
+            )
+        )
+    ]
+    own = (
+        pltpu.make_async_copy(latent_ref, latents.at[row, core, 0], own_sem.at[0]),
+        pltpu.make_async_copy(slots_ref.at[me], rows.at[row, core, 0], own_sem.at[1]),
+        pltpu.make_async_copy(tokens_ref, tokens.at[row, core], own_sem.at[2]),
+        pltpu.make_async_copy(query_ref, queries.at[row, core], own_sem.at[3]),
+    )
+    for copy in own:
+        copy.start()
+    greet(ep_count, me, head_index)
+
+    def latent_ep(step):
+        return remote(
+            latent_ref,
+            latents.at[row, core, step],
+            ep_send.at[1, step],
+            ep_recv.at[1, step],
+            (lax.rem(me + step, ep_count), head_index),
+        )
+
+    def slots_ep(step):
+        peer = lax.rem(me + step, ep_count)
+        return remote(
+            slots_ref.at[peer],
+            rows.at[row, core, step],
+            ep_send.at[0, step],
+            ep_recv.at[0, step],
+            (peer, head_index),
+        )
+
+    routes_of = {
+        "y": (row, y_send, y_recv, y_peer),
+        "core": (row, core_send, core_recv, core_peer),
+        "cross": (1 - row, cross_send, cross_recv, core_peer),
+    }
+
+    def moved(buffer, place, step, route):
+        origin_row, send_sem, recv_sem, device = routes_of[route]
+        block = buffer.at[origin_row, core] if step == ep_count else buffer.at[origin_row, core, step]
+        return remote(block, block, send_sem.at[place, step], recv_sem.at[place, step], device)
+
+    for step in range(1, ep_count):
+        latent_ep(step).start()
+    for step in range(1, ep_count):
+        slots_ep(step).start()
+    for copy in own:
+        copy.wait()
+    for route in ("y", "core"):
+        moved(queries, 1, ep_count, route).start()
+        moved(latents, 1, 0, route).start()
+        moved(tokens, 0, ep_count, route).start()
+    for fetch in fetches:
+        fetch.start()
+    for step in range(1, ep_count):
+        latent_ep(step).wait_recv()
+        for route in ("y", "core"):
+            moved(latents, 1, step, route).start()
+    moved(queries, 1, ep_count, "y").wait_recv()
+    moved(queries, 1, ep_count, "cross").start()
+    moved(tokens, 0, ep_count, "y").wait_recv()
+    moved(tokens, 0, ep_count, "cross").start()
+    for route in ("y", "core"):
+        moved(rows, 0, 0, route).start()
+    for step in range(ep_count):
+        moved(latents, 1, step, "y").wait_recv()
+        moved(latents, 1, step, "cross").start()
+    for route in ("core", "cross"):
+        moved(queries, 1, ep_count, route).wait_recv()
+        for step in range(ep_count):
+            moved(latents, 1, step, route).wait_recv()
+
+    rank_width = latent_columns_ref.shape[0]
+    head_lanes = attended.shape[1]
+    group_rows = attended.shape[0]
+    heads = head_lanes // VALUE
+
+    def project():
+        query_rows = queries[...].reshape(group_rows, queries.shape[-1])
+        projected = jnp.dot(
+            query_rows, query_columns_ref[...], preferred_element_type=jnp.float32
+        )
+        query_wide[:, :head_lanes] = projected[:, :head_lanes].astype(jnp.bfloat16)
+        turned = (
+            projected[:, head_lanes : head_lanes + 128] * turns_ref[0]
+            + projected[:, head_lanes + 128 :] * turns_ref[1]
+        )
+        query_wide[:, head_lanes:] = turned.astype(jnp.bfloat16)
+        for block in range(4):
+            packed = latents[block // 2, block % 2].reshape(ep_count * own_rows, latents.shape[-1])
+            expanded = jnp.dot(
+                packed[:, :rank_width],
+                latent_columns_ref[...],
+                preferred_element_type=jnp.float32,
+            ).astype(jnp.bfloat16)
+            span = slice(block * ep_count * own_rows, (block + 1) * ep_count * own_rows)
+            keys[span, :head_lanes] = expanded[:, :head_lanes]
+            keys[span, head_lanes:] = packed[:, rank_width:]
+            values[span, :] = expanded[:, head_lanes:]
+
+    def attend(block):
+        block_rows = group_rows // 4
+        span = slice(block * block_rows, (block + 1) * block_rows)
+        query_block = query_wide[span, :]
+        lane = lax.broadcasted_iota(jnp.int32, query_block.shape, 1)
+        lane_head = jnp.where(lane < head_lanes, lane // CONTENT, (lane - head_lanes) // ROTARY)
+        out_lane = lax.broadcasted_iota(jnp.int32, (block_rows, head_lanes), 1)
+        result = jnp.zeros((block_rows, head_lanes), jnp.float32)
+        for head in range(heads):
+            chosen = jnp.where(lane_head == head, query_block, jnp.zeros_like(query_block))
+            scores = lax.dot_general(
+                chosen, keys[...], (((1,), (1,)), ((), ())), preferred_element_type=jnp.float32
+            ) * ((CONTENT + ROTARY) ** (-0.5))
+            weights = jnp.exp(scores - jnp.max(scores, -1, keepdims=True))
+            total = jnp.sum(weights, -1, keepdims=True)
+            summed = jnp.dot(
+                weights.astype(jnp.bfloat16), values[...], preferred_element_type=jnp.float32
+            )
+            result = jnp.where(out_lane // VALUE == head, summed / total, result)
+        attended[span, :] = result.astype(jnp.bfloat16)
+
+    def mix():
+        for start in range(0, width, stripe):
+            product = jnp.dot(
+                attended[...],
+                output_weight_ref[:, start : start + stripe],
+                preferred_element_type=jnp.float32,
+            ).astype(jnp.bfloat16)
+            side[:, :, own_rows:, start : start + stripe] = product.reshape(
+                2, 2, own_rows, stripe
+            )
+
+    def share():
+        for fetch in fetches[:3]:
+            fetch.wait()
+        for route in ("core", "cross"):
+            moved(tokens, 0, ep_count, route).wait_recv()
+        hidden = gated_rows(
+            tokens[...].reshape(group_rows, width), shared_gate_ref[...], shared_up_ref[...]
+        )
+        for start in range(0, width, stripe):
+            product = jnp.dot(
+                hidden,
+                shared_down_ref[:, start : start + stripe],
+                preferred_element_type=jnp.float32,
+            ).astype(jnp.bfloat16)
+            side[:, :, :own_rows, start : start + stripe] = product.reshape(
+                2, 2, own_rows, stripe
+            )
+
+    def side_half(target_row, place):
+        return remote(
+            side.at[target_row, 1 - core],
+            half_side.at[target_row],
+            half_send.at[1, place],
+            half_recv.at[1, place],
+            core_peer,
+        )
+
+    near_side, outer_side = side_half(row, 0), side_half(1 - row, 1)
+    side_copy = remote(
+        side.at[1 - row, core], far_side, far_send.at[ep_count], far_recv.at[ep_count], y_peer
+    )
+
+    def side_exchange():
+        outer_side.start()
+        near_side.start()
+
+    def side_far():
+        outer_side.wait_recv()
+        side[1 - row, core] = (
+            side[1 - row, core].astype(jnp.float32) + half_side[1 - row].astype(jnp.float32)
+        ).astype(jnp.bfloat16)
+
+    tasks = [
+        project,
+        lambda: attend(0),
+        lambda: attend(1),
+        lambda: attend(2),
+        lambda: attend(3),
+        mix,
+        share,
+        side_exchange,
+        side_far,
+    ]
+    for step in range(max(ep_count + 1, len(tasks))):
+        if 0 < step < ep_count:
+            slots_ep(step).wait_recv()
+            for route in ("y", "core"):
+                moved(rows, 0, step, route).start()
+        if 0 < step <= ep_count:
+            moved(rows, 0, step - 1, "y").wait_recv()
+            moved(rows, 0, step - 1, "cross").start()
+        if step < len(tasks):
+            tasks[step]()
+    side_copy.start()
+    for fetch in fetches[3:]:
+        fetch.wait()
+    for route in ("core", "cross"):
+        for step in range(ep_count):
+            moved(rows, 0, step, route).wait_recv()
+
+    def compute(side_core):
+        for expert in range(local_experts):
+            span = slice(expert * capacity, (expert + 1) * capacity)
+            block = rows[:, side_core, :, span, :].reshape(2 * ep_count * capacity, width)
+            hidden = gated_rows(block, gate_ref[expert], up_ref[expert])
+            for start in range(0, width, stripe):
+                product = jnp.dot(
+                    hidden,
+                    down_ref[expert, :, start : start + stripe],
+                    preferred_element_type=jnp.float32,
+                ).astype(jnp.bfloat16)
+                part[:, side_core, :, span, start : start + stripe] = product.reshape(
+                    2, ep_count, capacity, stripe
+                )
+
+    def rows_half(target_row, place):
+        return remote(
+            part.at[target_row, 1 - core],
+            half_rows.at[target_row],
+            half_send.at[0, place],
+            half_recv.at[0, place],
+            core_peer,
+        )
+
+    compute(1 - core)
+    near, outer = rows_half(row, 0), rows_half(1 - row, 1)
+    outer.start()
+    near.start()
+    compute(core)
+
+    def y_copy(step):
+        return remote(
+            part.at[1 - row, core, step],
+            far_rows.at[step],
+            far_send.at[step],
+            far_recv.at[step],
+            y_peer,
+        )
+
+    def back_copy(step):
+        return remote(
+            part.at[row, core, step],
+            returned.at[me],
+            back_send.at[step],
+            back_recv.at[step],
+            (lax.rem(me + ep_count - step, ep_count), head_index),
+        )
+
+    outer.wait_recv()
+    order = list(range(1, ep_count)) + [0]
+    for step in order:
+        part[1 - row, core, step] = (
+            part[1 - row, core, step].astype(jnp.float32)
+            + half_rows[1 - row, step].astype(jnp.float32)
+        ).astype(jnp.bfloat16)
+        y_copy(step).start()
+    near.wait_recv()
+    near_side.wait_recv()
+    side_copy.wait_recv()
+    side_total = (
+        side[row, core].astype(jnp.float32)
+        + half_side[row].astype(jnp.float32)
+        + far_side[...].astype(jnp.float32)
+    )
+    mixer_out[...] = side_total[own_rows:].astype(jnp.bfloat16)
+    for step in order:
+        y_copy(step).wait_recv()
+        total = (
+            part[row, core, step].astype(jnp.float32)
+            + half_rows[row, step].astype(jnp.float32)
+            + far_rows[step].astype(jnp.float32)
+        ).astype(jnp.bfloat16)
+        if step > 0:
+            part[row, core, step] = total
+            back_copy(step).start()
+        else:
+            returned[me] = total
+    for step in range(1, ep_count):
+        back_copy(step).wait_recv()
+    for start in range(0, width, stripe):
+        picked = jnp.dot(
+            weight_ref[...],
+            returned[:, :, start : start + stripe].reshape(ep_count * slot_rows, stripe),
+            preferred_element_type=jnp.float32,
+        )
+        picked = picked[:own_rows] + picked[own_rows : 2 * own_rows] + picked[2 * own_rows :]
+        expert_out[:, start : start + stripe] = (
+            picked + side_total[:own_rows, start : start + stripe]
+        ).astype(jnp.bfloat16)
+
+    for step in range(1, ep_count):
+        latent_ep(step).wait_send()
+        slots_ep(step).wait_send()
+        back_copy(step).wait_send()
+    for route in ("y", "core", "cross"):
+        moved(queries, 1, ep_count, route).wait_send()
+        moved(tokens, 0, ep_count, route).wait_send()
+        for step in range(ep_count):
+            moved(latents, 1, step, route).wait_send()
+            moved(rows, 0, step, route).wait_send()
+    for copy in (near, outer, near_side, outer_side, side_copy):
+        copy.wait_send()
+    for step in range(ep_count):
+        y_copy(step).wait_send()
+
+
+def block_call(capacity, *operands):
+    slots, latent_pack, tokens, queries = operands[:4]
+    ep_count, slot_rows, width = slots.shape
+    own_rows = tokens.shape[0]
+    head_lanes = operands[7].shape[0]
+    vmem = pl.BlockSpec(memory_space=pltpu.VMEM)
+    anywhere = pl.BlockSpec(memory_space=pl.ANY)
+    out = jax.ShapeDtypeStruct((own_rows, width), jnp.bfloat16)
+
+    def held(*shape):
+        return pltpu.VMEM(shape, jnp.bfloat16)
+
+    def sems(*shape):
+        return pltpu.SemaphoreType.DMA(shape)
+
+    key_rows = 4 * ep_count * own_rows
+    return pl.pallas_call(
+        lambda *refs: block_kernel(ep_count, capacity, *refs),
+        out_shape=(out, out),
+        in_specs=[vmem] * 9 + [anywhere] * 6,
+        out_specs=(vmem, vmem),
+        scratch_shapes=[
+            held(2, 2, ep_count, slot_rows, width),
+            held(2, 2, ep_count, *latent_pack.shape),
+            held(2, 2, *tokens.shape),
+            held(2, 2, *queries.shape),
+        ]
+        + [held(*operand.shape) for operand in operands[9:]]
+        + [
+            held(key_rows, head_lanes + 128),
+            held(key_rows, head_lanes),
+            held(4 * own_rows, head_lanes + 128),
+            held(4 * own_rows, head_lanes),
+            held(2, 2, ep_count, slot_rows, width),
+            held(2, 2, 2 * own_rows, width),
+            held(2, ep_count, slot_rows, width),
+            held(2, 2 * own_rows, width),
+            held(ep_count, slot_rows, width),
+            held(2 * own_rows, width),
+            held(ep_count, slot_rows, width),
+        ]
+        + [sems(2, ep_count + 1)] * 8
+        + [
+            sems(4),
+            sems(6),
+            sems(2, 2),
+            sems(2, 2),
+            sems(ep_count + 1),
+            sems(ep_count + 1),
+            sems(ep_count),
+            sems(ep_count),
+        ],
+        compiler_params=pltpu.CompilerParams(
+            collective_id=0, has_side_effects=True, vmem_limit_bytes=VMEM_LIMIT
+        ),
+        name="block",
+    )(*operands)
+
+
+def shards(
+    query_latent,
+    key_latent,
+    rotary_key,
+    query_gain,
+    latent_gain,
+    query_content,
+    query_rotary,
+    key_content,
+    value_weight,
+    output_weight,
+    expert_input,
+    norm_gain,
+    routes,
+    route_weight,
+    expert_gate,
+    expert_up,
+    expert_down,
+    shared_gate,
+    shared_up,
+    shared_down,
+):
+    group_size = lax.axis_size("tp")
+    expert_groups = lax.axis_size("ep")
+    token_rows = expert_input.shape[0]
+    picks = routes.shape[1]
+    local_experts = expert_gate.shape[0]
+    expert_total = local_experts * expert_groups
+    capacity = 2 * token_rows * picks // expert_total
+    if group_size != 4 or capacity % 16:
+        return shards_plain(
+            query_latent,
+            key_latent,
+            rotary_key,
+            query_gain,
+            latent_gain,
+            query_content,
+            query_rotary,
+            key_content,
+            value_weight,
+            output_weight,
+            expert_input,
+            norm_gain,
+            routes,
+            route_weight,
+            expert_gate,
+            expert_up,
+            expert_down,
+            shared_gate,
+            shared_up,
+            shared_down,
+        )
+    own_rows = query_latent.shape[0]
+    head_local = HEADS // group_size
+    head_index = lax.axis_index("tp")
+    group_rows_count = own_rows * group_size
+    group_start = lax.axis_index("ep") * group_rows_count
+    own_start = group_start + head_index * own_rows
+    score_scale = (CONTENT + ROTARY) ** (-0.5)
+    query_normed = rms_rows(query_latent, query_gain).astype(jnp.bfloat16)
+    latent_normed = rms_rows(key_latent, latent_gain).astype(jnp.bfloat16)
+    own_positions = own_start + jnp.arange(own_rows, dtype=jnp.int32)
+    key_turned = turn_pairs(rotary_key.astype(jnp.float32)[:, None, :], own_positions)[
+        :, 0, :
+    ].astype(jnp.bfloat16)
+    slot_total = expert_total * capacity
+    model_width = expert_input.shape[1]
+    expert_normed = rms_rows(expert_input, norm_gain).astype(jnp.bfloat16)
+    flat_routes = routes.reshape(-1)
+    marks = (flat_routes[:, None] == jnp.arange(expert_total, dtype=jnp.int32)[None, :]).astype(
+        jnp.int32
+    )
+    ranks = jnp.sum((jnp.cumsum(marks, 0) - marks) * marks, 1)
+    targets = (flat_routes * capacity + ranks).reshape(token_rows, picks)
+    chosen = targets[:, :, None] == jnp.arange(slot_total, dtype=jnp.int32)[None, None, :]
+    picker = jnp.any(chosen, 1).astype(jnp.bfloat16)
+    spread_weight = jnp.sum(jnp.where(chosen, route_weight[:, :, None], 0.0), 1)
+    high = lax.reduce_precision(spread_weight, 8, 7)
+    middle = lax.reduce_precision(spread_weight - high, 8, 7)
+    low = spread_weight - high - middle
+    weight_terms = jnp.concatenate([high, middle, low], 0).astype(jnp.bfloat16)
+    slots = lax.dot_general(
+        picker, expert_normed, (((0,), (0,)), ((), ())), preferred_element_type=jnp.float32
+    ).astype(jnp.bfloat16)
+    slots = slots.reshape(expert_groups, local_experts * capacity, model_width)
+    latent_pack = jnp.concatenate(
+        [latent_normed]
+        + [key_turned] * head_local
+        + [jnp.zeros((own_rows, -head_local * ROTARY % 128), jnp.bfloat16)],
+        1,
+    )
+    content_columns = lax.dynamic_slice_in_dim(
+        query_content, head_index * head_local * CONTENT, head_local * CONTENT, 1
+    )
+    rotary_columns = lax.dynamic_slice_in_dim(
+        query_rotary, head_index * head_local * ROTARY, head_local * ROTARY, 1
+    )
+    paired = rotary_columns.reshape(-1, head_local * ROTARY // 2, 2)
+    swapped_columns = jnp.stack([-paired[:, :, 1], paired[:, :, 0]], -1).reshape(
+        rotary_columns.shape
+    )
+    lane_pad = ((0, 0), (0, -head_local * ROTARY % 128))
+    query_columns = jnp.concatenate(
+        [content_columns, jnp.pad(rotary_columns, lane_pad), jnp.pad(swapped_columns, lane_pad)], 1
+    )
+    key_columns = lax.dynamic_slice_in_dim(
+        key_content, head_index * head_local * CONTENT, head_local * CONTENT, 1
+    )
+    value_columns = lax.dynamic_slice_in_dim(
+        value_weight, head_index * head_local * VALUE, head_local * VALUE, 1
+    )
+    latent_columns = jnp.concatenate([key_columns, value_columns], 1)
+    positions = group_start + jnp.arange(group_rows_count, dtype=jnp.int32)
+    frequency = rope_base ** (-jnp.arange(ROTARY // 2, dtype=jnp.float32) * 2.0 / ROTARY)
+    angles = positions.astype(jnp.float32)[:, None] * jnp.tile(
+        jnp.repeat(frequency, 2), 128 // ROTARY
+    )[None, :]
+    turns = jnp.stack([jnp.cos(angles), jnp.sin(angles)])
+    return block_call(
+        capacity,
+        slots,
+        latent_pack,
+        expert_normed,
+        query_normed,
+        query_columns,
+        latent_columns,
+        turns,
+        output_weight,
+        weight_terms,
+        expert_gate,
+        expert_up,
+        expert_down,
+        shared_gate,
+        shared_up,
+        shared_down,
+    )
+
+
 def solution(mesh):
     in_specs = (
         P(("ep", "tp"), None),

time: 251 us -> 122 us (0.49)
  Pallas kernels: 0 us -> 99.3 us
  waiting for transfers between devices: 87.2 us -> 0 us
  blocking collectives: 80.8 us -> 0 us
  matrix products: 32 us -> 1.46 us
  between operations: 14.6 us -> 0.89 us
  local copies, waits for them, and re-layouts: 19.8 us -> 7.13 us
  starting transfers between devices: 5.76 us -> 0 us
  other arithmetic: 10.1 us -> 12.8 us
    pallas_call x0 -> x1, Pallas kernels: none -> 99.3 us  [block_call(): pl.pallas_call(lambda *refs: block_kernel(ep_count, capacity, *refs), out...]
    all_gather x4 -> x0, blocking collectives: 47.9 us -> none  [the longest x1 31.1 us: shards(): lax.all_gather(group_turn, 'ep', axis=0, tiled=True)]
    all_to_all x1 -> x0, blocking collectives: 32.8 us -> none  [shards(): lax.all_to_all(outgoing, 'ep', split_axis=0, concat_axis=0, tiled=True)]
    dot_general x13 -> x1, matrix products: 32 us -> 1.46 us  [shards(): lax.dot_general(picker, expert_normed, (((0,), (0,)), ((), ())), preferre...]
    all_gather x3 -> x0, waiting for transfers between devices: 26.7 us -> none  [the longest x1 26.7 us: shards(): lax.all_gather(received, 'tp', axis=0, tiled=True)]
    unnamed x7 -> x0, waiting for transfers between devices: 26.6 us -> none
    all_to_all x1 -> x0, waiting for transfers between devices: 20.1 us -> none  [shards(): lax.all_to_all(routed_sum.astype(jnp.bfloat16), 'ep', split_axis=0, conca...]
    reduce_scatter x2 -> x0, waiting for transfers between devices: 13.7 us -> none  [the longest x1 13.7 us: shards(): lax.psum_scatter(mixer_term.astype(jnp.bfloat16), 'tp', scatter_dimension...]
  transfers between devices with their start and end apart: 7 -> 0, of which waited for: 4 -> 0; matrix products, arithmetic and copies ran while one was open for 21% -> 0% of each run, Pallas kernels for 0% -> 0%
where the time goes in v2:
time: 122 us
  Pallas kernels  99.3 us (81%)
  other arithmetic  12.8 us (10%)
  local copies, waits for them, and re-layouts  7.13 us (6%)
  matrix products  1.46 us (1%)
    pallas_call x1, Pallas kernels, block_call(): pl.pallas_call(lambda *refs: block_kernel(ep_count, capacity, *refs), out...  99.3 us
    unnamed x11, local copies, waits for them, and re-layouts  4.13 us
    reduce_sum x3, other arithmetic, rms_rows(): jnp.mean(widened * widened, -1, keepdims=True) + norm_eps  2.99 us

profile of v2, /device:TPU:0, one launch (start us, length us, event | category | flops | bytes accessed | tf_op | source)
XLA Modules:
  0.0 121.6 jit_solution(16527377907514527922)
XLA Ops:
  0.7 1.0 fusion.8
  1.7 0.9 fusion.12
  2.6 1.1 fusion.3
  4.1 0.7 bitcast_convert_fusion
  5.1 0.8 fusion.14
  5.9 0.7 maximum_maximum_fusion.refs_1_
  6.6 0.8 copy.45
  7.5 1.5 %fusion.10.refs_3_ = bf16[64,512]{1,0:T(8,128)(2,1)} fusion(bf16[64,512]{1,0:T(8,128)(2,1)} %param.20, f32[512]{0:T(512)} %param.23, f32[64]{0:T(128)S(1)} %add_rsqrt_fusion), kind=kLoop, calls=%fused_computation.21 | loop fusion | flops 131072 | bytes 133376 | tf_op jit(solution)/shard_map/convert_element_type | solution.py:790
  9.1 0.2 reduce_window_sum.11
  9.3 0.2 select_reduce_fusion.1
  9.7 0.7 multiply_add_fusion
  10.5 0.8 select_reduce_fusion
  11.3 0.6 pad_maximum_fusion.2.refs_8_
  12.0 1.0 constant_dynamic-slice_fusion.1
  13.3 0.2 pad_maximum_fusion.3
  13.6 0.8 fusion.7.refs_4_
  14.5 0.9 constant_dynamic-slice_fusion
  15.4 0.7 pad_maximum_fusion.1.refs_5_
  16.0 0.5 multiply_cosine_fusion
  16.6 0.7 pad_maximum_fusion.refs_6_
  17.5 1.5 %convolution_convert_fusion = bf16[256,2048]{1,0:T(8,128)(2,1)} fusion(pred[64,256]{1,0:T(8,128)(4,1)S(1)} %fusion.11, bf16[64,2048]{1,0:T(8,128)(2,1)S(1)} %fusion.5.refs_2_), kind=kOutput, calls=%fused_computation | convolution fusion | flops 67633152 | bytes 1327104 | tf_op jit(solution)/shard_map/dot_general | solution.py:812
  18.9 99.3 %block.1 = (bf16[64,2048]{1,0:T(8,128)(2,1)}, bf16[64,2048]{1,0:T(8,128)(2,1)}) custom-call(bf16[8,32,2048]{2,1,0:T(8,128)(2,1)} %bitcast.15, bf16[64,384]{1,0:T(8,128)(2,1)} %maximum_maximum_fusion.refs_1_, bf16[64,2048]{1,0:T(8,128)(2,1)} %copy-done.1, bf16[64,512]{1,0:T(8,128)(2,1)} %fusion.10.refs_3_, bf16[512,384]{1,0:T(8,128)(2,1)} %fusion.7.refs_4_, ...), custom_call_target="tpu_custom_call" | custom-call | tf_op jit(solution)/shard_map/block/pallas_call | solution.py:688
  118.2 1.7 %copy.54 = bf16[64,2048]{1,0:T(8,128)(2,1)} copy(bf16[64,2048]{1,0:T(8,128)(2,1)} %get-tuple-element.15) | data formatting | bytes 524288
  119.9 1.7 %copy.55 = bf16[64,2048]{1,0:T(8,128)(2,1)} copy(bf16[64,2048]{1,0:T(8,128)(2,1)} %get-tuple-element.16) | data formatting | bytes 524288
  (39 shorter events, 1.8 us)
Async XLA Ops:
  0.6 13.0 %copy-start = (bf16[512,512]{1,0:T(8,128)(2,1)S(1)}, bf16[512,512]{1,0:T(8,128)(2,1)}, u32[]{:S(2)}) copy-start(bf16[512,512]{1,0:T(8,128)(2,1)} %param.25) | copy-start | bytes 1572868
  10.4 6.9 %copy-start.2 = (bf16[64,2048]{1,0:T(8,128)(2,1)S(1)}, bf16[64,2048]{1,0:T(8,128)(2,1)}, u32[]{:S(2)}) copy-start(bf16[64,2048]{1,0:T(8,128)(2,1)} %param.30) | copy-start | bytes 786436
  10.4 6.9 %copy-start.3 = (f32[2048]{0:T(1024)S(1)}, f32[2048]{0:T(1024)}, u32[]{:S(2)}) copy-start(f32[2048]{0:T(1024)} %param.31) | copy-start | bytes 24580
  17.4 1.5 %copy-start.1 = (bf16[64,2048]{1,0:T(8,128)(2,1)}, bf16[64,2048]{1,0:T(8,128)(2,1)S(1)}, u32[]{:S(2)}) copy-start(bf16[64,2048]{1,0:T(8,128)(2,1)S(1)} %fusion.5.refs_2_) | copy-start | bytes 786436

commit v3 on v2

--- a/solution.py
+++ b/solution.py
@@ -274,23 +274,34 @@
 def block_kernel(
     ep_count,
     capacity,
-    slots_ref,
-    latent_ref,
-    tokens_ref,
-    query_ref,
-    query_columns_ref,
-    latent_columns_ref,
-    turns_ref,
-    output_weight_ref,
-    weight_ref,
+    query_latent_ref,
+    key_latent_ref,
+    rotary_key_ref,
+    query_gain_ref,
+    latent_gain_ref,
+    expert_input_ref,
+    norm_gain_ref,
+    routes_ref,
+    route_weight_ref,
+    cosine_ref,
+    sine_ref,
+    query_content_hbm,
+    query_rotary_hbm,
+    key_content_hbm,
+    value_weight_hbm,
+    output_weight_hbm,
     gate_hbm,
     up_hbm,
     down_hbm,
     shared_gate_hbm,
     shared_up_hbm,
     shared_down_hbm,
-    mixer_out,
-    expert_out,
+    both_out,
+    slots_ref,
+    query_columns_ref,
+    latent_columns_ref,
+    output_weight_ref,
+    weight_ref,
     rows,
     latents,
     tokens,
@@ -350,10 +361,19 @@
             device_id_type=MESH,
         )
 
+    head_lanes = attended.shape[1]
+    heads = head_lanes // VALUE
+    columns = pl.ds(pl.multiple_of(head_index * head_lanes, head_lanes), head_lanes)
+    turn_columns = pl.ds(pl.multiple_of(head_index * heads * ROTARY // 128 * 128, 128), 128)
     fetches = [
         pltpu.make_async_copy(source, target, weight_sem.at[place])
         for place, (source, target) in enumerate(
             (
+                (query_content_hbm.at[:, columns], query_columns_ref.at[:, :head_lanes]),
+                (query_rotary_hbm.at[:, turn_columns], query_columns_ref.at[:, head_lanes:]),
+                (key_content_hbm.at[:, columns], latent_columns_ref.at[:, :head_lanes]),
+                (value_weight_hbm.at[:, columns], latent_columns_ref.at[:, head_lanes:]),
+                (output_weight_hbm, output_weight_ref),
                 (shared_gate_hbm, shared_gate_ref),
                 (shared_up_hbm, shared_up_ref),
                 (shared_down_hbm, shared_down_ref),
@@ -363,19 +383,37 @@
             )
         )
     ]
-    own = (
-        pltpu.make_async_copy(latent_ref, latents.at[row, core, 0], own_sem.at[0]),
-        pltpu.make_async_copy(slots_ref.at[me], rows.at[row, core, 0], own_sem.at[1]),
-        pltpu.make_async_copy(tokens_ref, tokens.at[row, core], own_sem.at[2]),
-        pltpu.make_async_copy(query_ref, queries.at[row, core], own_sem.at[3]),
-    )
-    for copy in own:
-        copy.start()
+    for fetch in fetches:
+        fetch.start()
+
+    def turn(entries, cosine, sine):
+        lane = lax.broadcasted_iota(jnp.int32, entries.shape, 1)
+        crossed = jnp.where(
+            lane % 2 == 0, -pltpu.roll(entries, 127, 1), pltpu.roll(entries, 1, 1)
+        )
+        return (entries * cosine + crossed * sine).astype(jnp.bfloat16)
+
+    latents[row, core, 0, :, : key_latent_ref.shape[1]] = rms_rows(
+        key_latent_ref[...], latent_gain_ref[...]
+    ).astype(jnp.bfloat16)
+    repeats = jnp.where(
+        lax.broadcasted_iota(jnp.int32, (ROTARY, 128), 0)
+        == lax.broadcasted_iota(jnp.int32, (ROTARY, 128), 1) % ROTARY,
+        1.0,
+        0.0,
+    ).astype(jnp.bfloat16)
+    own_span = pl.ds(pl.multiple_of(head_index * own_rows, own_rows), own_rows)
+    latents[row, core, 0, :, key_latent_ref.shape[1] :] = turn(
+        jnp.dot(rotary_key_ref[...], repeats, preferred_element_type=jnp.float32),
+        cosine_ref[own_span, :],
+        sine_ref[own_span, :],
+    )
+    queries[row, core] = rms_rows(query_latent_ref[...], query_gain_ref[...]).astype(jnp.bfloat16)
     greet(ep_count, me, head_index)
 
     def latent_ep(step):
         return remote(
-            latent_ref,
+            latents.at[row, core, 0],
             latents.at[row, core, step],
             ep_send.at[1, step],
             ep_recv.at[1, step],
@@ -405,16 +443,56 @@
 
     for step in range(1, ep_count):
         latent_ep(step).start()
-    for step in range(1, ep_count):
-        slots_ep(step).start()
-    for copy in own:
-        copy.wait()
     for route in ("y", "core"):
         moved(queries, 1, ep_count, route).start()
         moved(latents, 1, 0, route).start()
+    expert_normed = rms_rows(expert_input_ref[...], norm_gain_ref[...]).astype(jnp.bfloat16)
+    tokens[row, core] = expert_normed
+    for route in ("y", "core"):
         moved(tokens, 0, ep_count, route).start()
-    for fetch in fetches:
-        fetch.start()
+    expert_total = local_experts * ep_count
+    expert_lane = lax.broadcasted_iota(jnp.int32, (own_rows, expert_total), 1)
+    named = [
+        jnp.where(routes_ref[:, pick : pick + 1] == expert_lane, 1.0, 0.0)
+        for pick in range(routes_ref.shape[1])
+    ]
+    earlier = jnp.where(
+        lax.broadcasted_iota(jnp.int32, (own_rows, own_rows), 0)
+        > lax.broadcasted_iota(jnp.int32, (own_rows, own_rows), 1),
+        1.0,
+        0.0,
+    ).astype(jnp.bfloat16)
+    ahead = jnp.dot(earlier, sum(named).astype(jnp.bfloat16), preferred_element_type=jnp.float32)
+    slot_lane = lax.broadcasted_iota(jnp.int32, (own_rows, ep_count * slot_rows), 1)
+    picker = jnp.zeros(slot_lane.shape, jnp.float32)
+    weight = jnp.zeros(slot_lane.shape, jnp.float32)
+    for pick, marks in enumerate(named):
+        rank = jnp.sum(ahead * marks, 1, keepdims=True).astype(jnp.int32)
+        chosen = slot_lane == routes_ref[:, pick : pick + 1] * capacity + rank
+        picker = jnp.where(chosen, 1.0, picker)
+        weight = jnp.where(chosen, route_weight_ref[:, pick : pick + 1], weight)
+    high = weight.astype(jnp.bfloat16)
+    rest = weight - high.astype(jnp.float32)
+    middle = rest.astype(jnp.bfloat16)
+    weight_ref[:own_rows] = high
+    weight_ref[own_rows : 2 * own_rows] = middle
+    weight_ref[2 * own_rows :] = (rest - middle.astype(jnp.float32)).astype(jnp.bfloat16)
+    picker = picker.T.astype(jnp.bfloat16)
+    for start in range(0, width, stripe):
+        slots_ref[:, :, start : start + stripe] = (
+            jnp.dot(
+                picker, expert_normed[:, start : start + stripe], preferred_element_type=jnp.float32
+            )
+            .astype(jnp.bfloat16)
+            .reshape(ep_count, slot_rows, stripe)
+        )
+    for step in range(1, ep_count):
+        slots_ep(step).start()
+    own_slots = pltpu.make_async_copy(slots_ref.at[me], rows.at[row, core, 0], own_sem.at[0])
+    own_slots.start()
+    own_slots.wait()
+    for route in ("y", "core"):
+        moved(rows, 0, 0, route).start()
     for step in range(1, ep_count):
         latent_ep(step).wait_recv()
         for route in ("y", "core"):
@@ -423,8 +501,6 @@
     moved(queries, 1, ep_count, "cross").start()
     moved(tokens, 0, ep_count, "y").wait_recv()
     moved(tokens, 0, ep_count, "cross").start()
-    for route in ("y", "core"):
-        moved(rows, 0, 0, route).start()
     for step in range(ep_count):
         moved(latents, 1, step, "y").wait_recv()
         moved(latents, 1, step, "cross").start()
@@ -434,21 +510,19 @@
             moved(latents, 1, step, route).wait_recv()
 
     rank_width = latent_columns_ref.shape[0]
-    head_lanes = attended.shape[1]
     group_rows = attended.shape[0]
-    heads = head_lanes // VALUE
 
     def project():
+        for fetch in fetches[:5]:
+            fetch.wait()
         query_rows = queries[...].reshape(group_rows, queries.shape[-1])
         projected = jnp.dot(
             query_rows, query_columns_ref[...], preferred_element_type=jnp.float32
         )
         query_wide[:, :head_lanes] = projected[:, :head_lanes].astype(jnp.bfloat16)
-        turned = (
-            projected[:, head_lanes : head_lanes + 128] * turns_ref[0]
-            + projected[:, head_lanes + 128 :] * turns_ref[1]
-        )
-        query_wide[:, head_lanes:] = turned.astype(jnp.bfloat16)
+        query_wide[:, head_lanes:] = turn(
+            projected[:, head_lanes:], cosine_ref[...], sine_ref[...]
+        )
         for block in range(4):
             packed = latents[block // 2, block % 2].reshape(ep_count * own_rows, latents.shape[-1])
             expanded = jnp.dot(
@@ -466,7 +540,11 @@
         span = slice(block * block_rows, (block + 1) * block_rows)
         query_block = query_wide[span, :]
         lane = lax.broadcasted_iota(jnp.int32, query_block.shape, 1)
-        lane_head = jnp.where(lane < head_lanes, lane // CONTENT, (lane - head_lanes) // ROTARY)
+        lane_head = jnp.where(
+            lane < head_lanes,
+            lane // CONTENT,
+            (lane - head_lanes) // ROTARY - head_index * heads % (128 // ROTARY),
+        )
         out_lane = lax.broadcasted_iota(jnp.int32, (block_rows, head_lanes), 1)
         result = jnp.zeros((block_rows, head_lanes), jnp.float32)
         for head in range(heads):
@@ -494,7 +572,7 @@
             )
 
     def share():
-        for fetch in fetches[:3]:
+        for fetch in fetches[5:8]:
             fetch.wait()
         for route in ("core", "cross"):
             moved(tokens, 0, ep_count, route).wait_recv()
@@ -557,7 +635,7 @@
         if step < len(tasks):
             tasks[step]()
     side_copy.start()
-    for fetch in fetches[3:]:
+    for fetch in fetches[8:]:
         fetch.wait()
     for route in ("core", "cross"):
         for step in range(ep_count):
@@ -627,7 +705,7 @@
         + half_side[row].astype(jnp.float32)
         + far_side[...].astype(jnp.float32)
     )
-    mixer_out[...] = side_total[own_rows:].astype(jnp.bfloat16)
+    both_out[0] = side_total[own_rows:]
     for step in order:
         y_copy(step).wait_recv()
         total = (
@@ -649,9 +727,9 @@
             preferred_element_type=jnp.float32,
         )
         picked = picked[:own_rows] + picked[own_rows : 2 * own_rows] + picked[2 * own_rows :]
-        expert_out[:, start : start + stripe] = (
+        both_out[1, :, start : start + stripe] = (
             picked + side_total[:own_rows, start : start + stripe]
-        ).astype(jnp.bfloat16)
+        )
 
     for step in range(1, ep_count):
         latent_ep(step).wait_send()
@@ -669,14 +747,14 @@
         y_copy(step).wait_send()
 
 
-def block_call(capacity, *operands):
-    slots, latent_pack, tokens, queries = operands[:4]
-    ep_count, slot_rows, width = slots.shape
-    own_rows = tokens.shape[0]
-    head_lanes = operands[7].shape[0]
+def block_call(ep_count, capacity, *operands):
+    query_latent, key_latent = operands[:2]
+    own_rows, width = operands[5].shape
+    head_lanes = operands[15].shape[0]
+    slot_rows = operands[16].shape[0] * capacity
+    latent_shape = (own_rows, key_latent.shape[1] + 128)
     vmem = pl.BlockSpec(memory_space=pltpu.VMEM)
     anywhere = pl.BlockSpec(memory_space=pl.ANY)
-    out = jax.ShapeDtypeStruct((own_rows, width), jnp.bfloat16)
 
     def held(*shape):
         return pltpu.VMEM(shape, jnp.bfloat16)
@@ -687,16 +765,21 @@
     key_rows = 4 * ep_count * own_rows
     return pl.pallas_call(
         lambda *refs: block_kernel(ep_count, capacity, *refs),
-        out_shape=(out, out),
-        in_specs=[vmem] * 9 + [anywhere] * 6,
-        out_specs=(vmem, vmem),
+        out_shape=jax.ShapeDtypeStruct((2, own_rows, width), jnp.float32),
+        in_specs=[vmem] * 11 + [anywhere] * 11,
+        out_specs=vmem,
         scratch_shapes=[
+            held(ep_count, slot_rows, width),
+            held(query_latent.shape[1], head_lanes + 128),
+            held(key_latent.shape[1], 2 * head_lanes),
+            held(head_lanes, width),
+            held(3 * own_rows, ep_count * slot_rows),
             held(2, 2, ep_count, slot_rows, width),
-            held(2, 2, ep_count, *latent_pack.shape),
-            held(2, 2, *tokens.shape),
-            held(2, 2, *queries.shape),
+            held(2, 2, ep_count, *latent_shape),
+            held(2, 2, own_rows, width),
+            held(2, 2, *query_latent.shape),
         ]
-        + [held(*operand.shape) for operand in operands[9:]]
+        + [held(*operand.shape) for operand in operands[16:]]
         + [
             held(key_rows, head_lanes + 128),
             held(key_rows, head_lanes),
@@ -712,8 +795,8 @@
         ]
         + [sems(2, ep_count + 1)] * 8
         + [
-            sems(4),
-            sems(6),
+            sems(1),
+            sems(11),
             sems(2, 2),
             sems(2, 2),
             sems(ep_count + 1),
@@ -780,83 +863,33 @@
             shared_up,
             shared_down,
         )
-    own_rows = query_latent.shape[0]
-    head_local = HEADS // group_size
-    head_index = lax.axis_index("tp")
-    group_rows_count = own_rows * group_size
-    group_start = lax.axis_index("ep") * group_rows_count
-    own_start = group_start + head_index * own_rows
-    score_scale = (CONTENT + ROTARY) ** (-0.5)
-    query_normed = rms_rows(query_latent, query_gain).astype(jnp.bfloat16)
-    latent_normed = rms_rows(key_latent, latent_gain).astype(jnp.bfloat16)
-    own_positions = own_start + jnp.arange(own_rows, dtype=jnp.int32)
-    key_turned = turn_pairs(rotary_key.astype(jnp.float32)[:, None, :], own_positions)[
-        :, 0, :
-    ].astype(jnp.bfloat16)
-    slot_total = expert_total * capacity
-    model_width = expert_input.shape[1]
-    expert_normed = rms_rows(expert_input, norm_gain).astype(jnp.bfloat16)
-    flat_routes = routes.reshape(-1)
-    marks = (flat_routes[:, None] == jnp.arange(expert_total, dtype=jnp.int32)[None, :]).astype(
-        jnp.int32
-    )
-    ranks = jnp.sum((jnp.cumsum(marks, 0) - marks) * marks, 1)
-    targets = (flat_routes * capacity + ranks).reshape(token_rows, picks)
-    chosen = targets[:, :, None] == jnp.arange(slot_total, dtype=jnp.int32)[None, None, :]
-    picker = jnp.any(chosen, 1).astype(jnp.bfloat16)
-    spread_weight = jnp.sum(jnp.where(chosen, route_weight[:, :, None], 0.0), 1)
-    high = lax.reduce_precision(spread_weight, 8, 7)
-    middle = lax.reduce_precision(spread_weight - high, 8, 7)
-    low = spread_weight - high - middle
-    weight_terms = jnp.concatenate([high, middle, low], 0).astype(jnp.bfloat16)
-    slots = lax.dot_general(
-        picker, expert_normed, (((0,), (0,)), ((), ())), preferred_element_type=jnp.float32
-    ).astype(jnp.bfloat16)
-    slots = slots.reshape(expert_groups, local_experts * capacity, model_width)
-    latent_pack = jnp.concatenate(
-        [latent_normed]
-        + [key_turned] * head_local
-        + [jnp.zeros((own_rows, -head_local * ROTARY % 128), jnp.bfloat16)],
-        1,
-    )
-    content_columns = lax.dynamic_slice_in_dim(
-        query_content, head_index * head_local * CONTENT, head_local * CONTENT, 1
-    )
-    rotary_columns = lax.dynamic_slice_in_dim(
-        query_rotary, head_index * head_local * ROTARY, head_local * ROTARY, 1
-    )
-    paired = rotary_columns.reshape(-1, head_local * ROTARY // 2, 2)
-    swapped_columns = jnp.stack([-paired[:, :, 1], paired[:, :, 0]], -1).reshape(
-        rotary_columns.shape
-    )
-    lane_pad = ((0, 0), (0, -head_local * ROTARY % 128))
-    query_columns = jnp.concatenate(
-        [content_columns, jnp.pad(rotary_columns, lane_pad), jnp.pad(swapped_columns, lane_pad)], 1
-    )
-    key_columns = lax.dynamic_slice_in_dim(
-        key_content, head_index * head_local * CONTENT, head_local * CONTENT, 1
-    )
-    value_columns = lax.dynamic_slice_in_dim(
-        value_weight, head_index * head_local * VALUE, head_local * VALUE, 1
-    )
-    latent_columns = jnp.concatenate([key_columns, value_columns], 1)
-    positions = group_start + jnp.arange(group_rows_count, dtype=jnp.int32)
+    group_rows_count = expert_input.shape[0] * group_size
+    positions = lax.axis_index("ep") * group_rows_count + jnp.arange(
+        group_rows_count, dtype=jnp.int32
+    )
     frequency = rope_base ** (-jnp.arange(ROTARY // 2, dtype=jnp.float32) * 2.0 / ROTARY)
     angles = positions.astype(jnp.float32)[:, None] * jnp.tile(
         jnp.repeat(frequency, 2), 128 // ROTARY
     )[None, :]
-    turns = jnp.stack([jnp.cos(angles), jnp.sin(angles)])
-    return block_call(
+    both = block_call(
+        expert_groups,
         capacity,
-        slots,
-        latent_pack,
-        expert_normed,
-        query_normed,
-        query_columns,
-        latent_columns,
-        turns,
+        query_latent,
+        key_latent,
+        rotary_key,
+        query_gain[None, :],
+        latent_gain[None, :],
+        expert_input,
+        norm_gain[None, :],
+        routes,
+        route_weight,
+        jnp.cos(angles),
+        jnp.sin(angles),
+        query_content,
+        query_rotary,
+        key_content,
+        value_weight,
         output_weight,
-        weight_terms,
         expert_gate,
         expert_up,
         expert_down,
@@ -864,6 +897,7 @@
         shared_up,
         shared_down,
     )
+    return (both[0].astype(jnp.bfloat16), both[1].astype(jnp.bfloat16))
 
 
 def solution(mesh):

time: 122 us -> 109 us (0.89)
  other arithmetic: 12.8 us -> 2.53 us
  local copies, waits for them, and re-layouts: 7.13 us -> 5.22 us
  matrix products: 1.46 us -> 0 us
    reduce_sum x5 -> x0, other arithmetic: 3.95 us -> none  [the longest x3 2.99 us: rms_rows(): jnp.mean(widened * widened, -1, keepdims=True) + norm_eps]
    concatenate x4 -> x0, other arithmetic: 2.84 us -> none  [the longest x1 0.83 us: shards(): jnp.concatenate([content_columns, jnp.pad(rotary_columns, lane_pad), jnp....]
    convert_element_type x5 -> x0, other arithmetic: 2.6 us -> none  [the longest x1 1.54 us: shards(): query_normed = rms_rows(query_latent, query_gain).astype(jnp.bfloat16)]
    dynamic_slice x4 -> x0, local copies, waits for them, and re-layouts: 2.01 us -> none  [the longest x2 1.1 us: shards(): lax.dynamic_slice_in_dim(query_rotary, head_index * head_local * ROTARY,...]
    dot_general x1 -> x0, matrix products: 1.46 us -> none  [shards(): lax.dot_general(picker, expert_normed, (((0,), (0,)), ((), ())), preferre...]
    sin x0 -> x1, other arithmetic: none -> 1.23 us  [shards(): jnp.sin(angles)]
    unnamed x11 -> x3, local copies, waits for them, and re-layouts: 4.13 us -> 4.14 us
where the time goes in v3:
time: 109 us; the launch traced here: 108 us
  Pallas kernels  99.9 us (92%)
  local copies, waits for them, and re-layouts  5.22 us (5%)
  other arithmetic  2.53 us (2%)
    pallas_call x1, Pallas kernels, block_call(): pl.pallas_call(lambda *refs: block_kernel(ep_count, capacity, *refs), out...  99.9 us
    unnamed x3, local copies, waits for them, and re-layouts  4.14 us

profile of v3, /device:TPU:0, one launch (start us, length us, event | category | flops | bytes accessed | tf_op | source)
XLA Modules:
  0.0 108.3 jit_solution(14237951319313438777)
XLA Ops:
  0.7 0.1 broadcast_in_dim.16
  0.7 0.1 tile.7
  0.8 0.1 mul.21
  0.9 1.4 %copy.25.refs_2_ = bf16[64,32]{1,0:T(8,128)(2,1)} copy(bf16[64,32]{0,1:T(8,128)(2,1)} %param.22) | data formatting | bytes 8192 | tf_op args[2]
  2.3 1.4 %copy.26.refs_7_ = s32[64,2]{1,0:T(8,128)} copy(s32[64,2]{0,1:T(2,128)} %param.32) | data formatting | bytes 1024 | tf_op args[12]
  3.7 1.4 %copy.27.refs_8_ = f32[64,2]{1,0:T(8,128)} copy(f32[64,2]{0,1:T(2,128)} %param.33) | data formatting | bytes 1024 | tf_op args[13]
  5.1 1.2 %multiply_sine_fusion = (f32[256,128]{1,0:T(8,128)}, f32[256,128]{1,0:T(8,128)}) fusion(f32[128]{0:T(128)S(1)} %mul.21, f32[256]{0:T(256)S(1)} %add_convert_fusion), kind=kLoop, calls=%fused_computation.2 | loop fusion | flops 32768 | bytes 263680 | tf_op jit(solution)/shard_map/sin | solution.py:887
  6.3 99.9 %block.1 = f32[2,64,2048]{2,1,0:T(8,128)} custom-call(bf16[64,512]{1,0:T(8,128)(2,1)} %refs_0_.1, bf16[64,256]{1,0:T(8,128)(2,1)} %refs_1_.1, bf16[64,32]{1,0:T(8,128)(2,1)} %copy.25.refs_2_, f32[1,512]{1,0:T(1,128)} %bitcast.8, f32[1,256]{1,0:T(1,128)} %bitcast.9, bf16[64,2048]{1,0:T(8,128)(2,1)} %refs_5_.1, f32[1,2048]{1,0:T(1,128)} %bitcast.7, ...), custom_call_target="tpu_custom_call" | custom-call | tf_op jit(solution)/shard_map/block/pallas_call | solution.py:766
  106.2 1.3 %convert.4 = bf16[2,64,2048]{2,1,0:T(8,128)(2,1)S(1)} convert(f32[2,64,2048]{2,1,0:T(8,128)} %block.1) | non-fusion elementwise | flops 262144 | bytes 1572864 | tf_op jit(solution)/shard_map/convert.1
  107.5 0.8 slice_bitcast_fusion
  (3 shorter events, 0.0 us)

commit v4 on v3

--- a/solution.py
+++ b/solution.py
@@ -404,7 +404,12 @@
     ).astype(jnp.bfloat16)
     own_span = pl.ds(pl.multiple_of(head_index * own_rows, own_rows), own_rows)
     latents[row, core, 0, :, key_latent_ref.shape[1] :] = turn(
-        jnp.dot(rotary_key_ref[...], repeats, preferred_element_type=jnp.float32),
+        lax.dot_general(
+            rotary_key_ref[...],
+            repeats,
+            (((0,), (0,)), ((), ())),
+            preferred_element_type=jnp.float32,
+        ),
         cosine_ref[own_span, :],
         sine_ref[own_span, :],
     )
@@ -452,9 +457,11 @@
         moved(tokens, 0, ep_count, route).start()
     expert_total = local_experts * ep_count
     expert_lane = lax.broadcasted_iota(jnp.int32, (own_rows, expert_total), 1)
+    route_columns = routes_ref[...].T
+    weight_columns = route_weight_ref[...].T
     named = [
-        jnp.where(routes_ref[:, pick : pick + 1] == expert_lane, 1.0, 0.0)
-        for pick in range(routes_ref.shape[1])
+        jnp.where(route_columns[:, pick : pick + 1] == expert_lane, 1.0, 0.0)
+        for pick in range(routes_ref.shape[0])
     ]
     earlier = jnp.where(
         lax.broadcasted_iota(jnp.int32, (own_rows, own_rows), 0)
@@ -468,9 +475,9 @@
     weight = jnp.zeros(slot_lane.shape, jnp.float32)
     for pick, marks in enumerate(named):
         rank = jnp.sum(ahead * marks, 1, keepdims=True).astype(jnp.int32)
-        chosen = slot_lane == routes_ref[:, pick : pick + 1] * capacity + rank
+        chosen = slot_lane == route_columns[:, pick : pick + 1] * capacity + rank
         picker = jnp.where(chosen, 1.0, picker)
-        weight = jnp.where(chosen, route_weight_ref[:, pick : pick + 1], weight)
+        weight = jnp.where(chosen, weight_columns[:, pick : pick + 1], weight)
     high = weight.astype(jnp.bfloat16)
     rest = weight - high.astype(jnp.float32)
     middle = rest.astype(jnp.bfloat16)
@@ -705,7 +712,7 @@
         + half_side[row].astype(jnp.float32)
         + far_side[...].astype(jnp.float32)
     )
-    both_out[0] = side_total[own_rows:]
+    both_out[0] = side_total[own_rows:].astype(jnp.bfloat16)
     for step in order:
         y_copy(step).wait_recv()
         total = (
@@ -729,7 +736,7 @@
         picked = picked[:own_rows] + picked[own_rows : 2 * own_rows] + picked[2 * own_rows :]
         both_out[1, :, start : start + stripe] = (
             picked + side_total[:own_rows, start : start + stripe]
-        )
+        ).astype(jnp.bfloat16)
 
     for step in range(1, ep_count):
         latent_ep(step).wait_send()
@@ -765,7 +772,7 @@
     key_rows = 4 * ep_count * own_rows
     return pl.pallas_call(
         lambda *refs: block_kernel(ep_count, capacity, *refs),
-        out_shape=jax.ShapeDtypeStruct((2, own_rows, width), jnp.float32),
+        out_shape=jax.ShapeDtypeStruct((2, own_rows, width), jnp.bfloat16),
         in_specs=[vmem] * 11 + [anywhere] * 11,
         out_specs=vmem,
         scratch_shapes=[
@@ -876,13 +883,13 @@
         capacity,
         query_latent,
         key_latent,
-        rotary_key,
+        rotary_key.T,
         query_gain[None, :],
         latent_gain[None, :],
         expert_input,
         norm_gain[None, :],
-        routes,
-        route_weight,
+        routes.T,
+        route_weight.T,
         jnp.cos(angles),
         jnp.sin(angles),
         query_content,
@@ -897,7 +904,7 @@
         shared_up,
         shared_down,
     )
-    return (both[0].astype(jnp.bfloat16), both[1].astype(jnp.bfloat16))
+    return (both[0], both[1])
 
 
 def solution(mesh):

time: 109 us -> 104 us (0.954)
  local copies, waits for them, and re-layouts: 5.22 us -> 2.11 us
  other arithmetic: 2.53 us -> 1.25 us
    unnamed x3 -> x0, local copies, waits for them, and re-layouts: 4.14 us -> none
    squeeze x0 -> x1, local copies, waits for them, and re-layouts: none -> 1.87 us  [shards(): return (both[0], both[1])]
    another operation x1 -> x0, other arithmetic: 1.28 us -> none
where the time goes in v4:
time: 104 us
  Pallas kernels  99.7 us (96%)
  local copies, waits for them, and re-layouts  2.11 us (2%)
  other arithmetic  1.25 us (1%)
    pallas_call x1, Pallas kernels, block_call(): pl.pallas_call(lambda *refs: block_kernel(ep_count, capacity, *refs), out...  99.7 us

profile of v4, /device:TPU:0, one launch (start us, length us, event | category | flops | bytes accessed | tf_op | source)
XLA Modules:
  0.0 103.8 jit_solution(753067209127568395)
XLA Ops:
  0.7 0.1 broadcast_in_dim.16
  0.7 0.1 tile.7
  0.8 0.1 mul.21
  0.9 1.2 %multiply_sine_fusion = (f32[256,128]{1,0:T(8,128)}, f32[256,128]{1,0:T(8,128)}) fusion(f32[128]{0:T(128)S(1)} %mul.21, f32[256]{0:T(256)S(1)} %add_convert_fusion), kind=kLoop, calls=%fused_computation.2 | loop fusion | flops 32768 | bytes 263680 | tf_op jit(solution)/shard_map/sin | solution.py:894
  2.2 99.7 %block.1 = bf16[2,64,2048]{2,1,0:T(8,128)(2,1)} custom-call(bf16[64,512]{1,0:T(8,128)(2,1)} %refs_0_.1, bf16[64,256]{1,0:T(8,128)(2,1)} %refs_1_.1, bf16[32,64]{1,0:T(8,128)(2,1)} %bitcast.10, f32[1,512]{1,0:T(1,128)} %bitcast.12, f32[1,256]{1,0:T(1,128)} %bitcast.13, bf16[64,2048]{1,0:T(8,128)(2,1)} %refs_5_.1, f32[1,2048]{1,0:T(1,128)} %bitcast.11, ...), custom_call_target="tpu_custom_call" | custom-call | tf_op jit(solution)/shard_map/block/pallas_call | solution.py:773
  101.9 1.9 %slice_bitcast_fusion = (bf16[64,2048]{1,0:T(8,128)(2,1)}, bf16[64,2048]{1,0:T(8,128)(2,1)}) fusion(bf16[2,64,2048]{2,1,0:T(8,128)(2,1)} %block.1), kind=kLoop, calls=%fused_computation | loop fusion | bytes 1048576 | tf_op jit(solution)/shard_map/squeeze | solution.py:907
  (3 shorter events, 0.0 us)
